TPU v7x, 512 devices: a whole 4x4x16 slice. The times are simulated.
512 devices in a mesh: ep: 32 (over z, core), tp: 16 (over y, x).
Axes of the slice: x: 4, y: 4, z: 16, core: 2. Of those that a mesh axis runs over, the one named last changes fastest.
Arguments:
- mixer_value_input: bfloat16 [8192, 4096], P('ep', 'tp'), may hold values from -6 to 6
- input_state_matrix: bfloat16 [8192, 2048], P('ep', 'tp'), may hold values from -6 to 6
- output_state_matrix: bfloat16 [8192, 2048], P('ep', 'tp'), may hold values from -6 to 6
- output_gate_input: bfloat16 [8192, 4096], P('ep', 'tp'), may hold values from -6 to 6
- step_input: float32 [8192, 64], P('ep', 'tp'), may hold values from -6 to -2
- extra_log_decay: float32 [8192, 64], P('ep', 'tp'), may hold values from -1 to 0
- head_log_decay: float32 [64], P('tp'), may hold values from -10 to 1
- head_skip_scale: float32 [64], P('tp'), may hold values from 0.5 to 2
- value_kernel: float32 [4, 4096], P(None, 'tp'), may hold values from -3 to 3
- input_matrix_kernel: float32 [4, 2048], P(None, 'tp'), may hold values from -3 to 3
- output_matrix_kernel: float32 [4, 2048], P(None, 'tp'), may hold values from -3 to 3
- mixer_norm_scale: float32 [4096], P('tp'), may hold values from 0.1 to 1.9
- mixer_output_weight: bfloat16 [4096, 2048], P(None, 'tp'), may hold values from -0.09375 to 0.09375
- second_token_rows: bfloat16 [8192, 2048], P('ep'), may hold values from -6 to 6
- expert_norm_scale: float32 [2048], replicated, may hold values from 0.1 to 1.9
- routed_expert_index: int32 [8192, 4], P('ep'), may hold values from 0 to 63, all different within a row; in each aligned block of 256 rows (0 to 255, 256 to 511, ...) at most 24 rows name the same one
- routed_expert_weight: float32 [8192, 4], P('ep'), may hold values from 0.1 to 1
- routed_gate_weight: bfloat16 [64, 2048, 1024], P('ep', None, 'tp'), may hold values from -0.125 to 0.125
- routed_up_weight: bfloat16 [64, 2048, 1024], P('ep', None, 'tp'), may hold values from -0.125 to 0.125
- routed_down_weight: bfloat16 [64, 1024, 2048], P('ep', None, 'tp'), may hold values from -0.1875 to 0.1875
- shared_gate_weight: bfloat16 [2048, 1024], P(None, 'tp'), may hold values from -0.125 to 0.125
- shared_up_weight: bfloat16 [2048, 1024], P(None, 'tp'), may hold values from -0.125 to 0.125
- shared_down_weight: bfloat16 [1024, 2048], P(None, 'tp'), may hold values from -0.1875 to 0.1875
Outputs:
- mixer_output: bfloat16 [8192, 2048], P('ep', 'tp')
- routed_out: bfloat16 [8192, 2048], P('ep', 'tp')
Inputs may be any that keep to these rules, and one draw needn't show every extreme that they name: `routed_expert_index`: in each aligned block of 256 rows (the rows of one index of ep) no expert is named more than 24 times, a bound that some block reaches.
All inputs are finite; a program needn't handle non-finite values.
Results may differ from a plain program's by a relative error of at most 0.012.
Values may be sent and summed in bfloat16 or wider, within the bound.
No kernel may reach another device: no remote copies, remote signals or barrier semaphores. Data moves between devices by JAX's collectives and lax.ppermute only.
A program may use at most 64 MiB of HBM per device.

v0:
```python
import jax
import jax.numpy as jnp
from jax import lax
from jax.sharding import PartitionSpec as P

HEAD_DIM = 64
STATE = 128
CONV_TAPS = 4
BLOCK = 128
TOP_K = 4


epsilon = 1e-05


def passed_along(x, axis, by):
    size = lax.axis_size(axis)
    pairs = [(i, i + by) for i in range(size) if 0 <= i + by < size]
    return lax.ppermute(x, axis, pairs)


def carried_in(x, axis, join, neutral):
    place = lax.axis_index(axis)
    gathered = jax.tree.map(
        lambda a, kind: lax.all_gather(a.astype(kind), axis), x, (jnp.bfloat16, jnp.bfloat16)
    )
    state = jax.tree.map(lambda a, e: jnp.zeros_like(a) + jnp.asarray(e, a.dtype), x, neutral)

    def one(turn, state):
        return join(
            state,
            jax.tree.map(
                lambda a, own: lax.dynamic_index_in_dim(a, turn, 0, False).astype(own.dtype),
                gathered,
                x,
            ),
        )

    return lax.fori_loop(0, place, one, state)


def laid_out(tiles, dim):
    tiles = jnp.moveaxis(tiles, 0, dim)
    dims = tiles.shape
    return tiles.reshape(*dims[:dim], dims[dim] * dims[dim + 1], *dims[dim + 2 :])


def one_gather(arrays, axis, dims):
    ravelled = jnp.concatenate([a.reshape(-1) for a in arrays])
    lines, at, finished = (lax.all_gather(ravelled, axis), 0, [])
    for a, dim in zip(arrays, dims):
        tiles = lines[:, at : at + a.size].reshape(-1, *a.shape)
        finished.append(laid_out(tiles, dim))
        at += a.size
    return tuple(finished)


def conv_silu(tail_rows, source, weights):
    length = source.shape[0]
    padded = jnp.concatenate([tail_rows, source], axis=0)
    total_sum = jnp.zeros(source.shape, jnp.float32)
    for tap_index in range(CONV_TAPS):
        total_sum = (
            total_sum
            + padded[tap_index : tap_index + length].astype(jnp.float32) * weights[tap_index]
        )
    return jax.nn.silu(total_sum).astype(jnp.bfloat16)


def join_states(earlier, later_part):
    return (earlier[0] * later_part[0], later_part[0][:, None, None] * earlier[1] + later_part[1])


def carry_blocks(carried, inputs):
    block_decay, block_state = inputs
    return (carried * block_decay[:, None, None] + block_state, carried)


def route_slots(route_block, experts, capacity):
    flat_ids = route_block.reshape(-1)
    onehot = (flat_ids[:, None] == jnp.arange(experts, dtype=jnp.int32)[None, :]).astype(jnp.int32)
    earlier = jnp.cumsum(onehot, axis=0) - onehot
    position_in = jnp.sum(earlier * onehot, axis=1)
    slot_index = flat_ids * capacity + position_in
    owner_row = jnp.arange(flat_ids.shape[0], dtype=jnp.int32) // route_block.shape[1]
    slot_owner = (
        jnp.full((experts * capacity,), route_block.shape[0], jnp.int32)
        .at[slot_index]
        .set(owner_row)
    )
    return (slot_owner, slot_index)


def on_device(
    mixer_value_input,
    input_state_matrix,
    output_state_matrix,
    output_gate_input,
    step_input,
    extra_log_decay,
    head_log_decay,
    head_skip_scale,
    value_kernel,
    input_matrix_kernel,
    output_matrix_kernel,
    mixer_norm_scale,
    mixer_output_weight,
    second_token_rows,
    expert_norm_scale,
    routed_expert_index,
    routed_expert_weight,
    routed_gate_weight,
    routed_up_weight,
    routed_down_weight,
    shared_gate_weight,
    shared_up_weight,
    shared_down_weight,
):
    length = mixer_value_input.shape[0]
    heads_local = step_input.shape[1]
    width_x = mixer_value_input.shape[1]
    width_b = input_state_matrix.shape[1]
    groups_local = width_b // STATE
    head_ratio = heads_local // groups_local
    nblocks = length // BLOCK
    lead_row = length - CONV_TAPS + 1
    edge_rows = jnp.concatenate(
        [
            mixer_value_input[lead_row:],
            input_state_matrix[lead_row:],
            output_state_matrix[lead_row:],
        ],
        axis=1,
    )
    tail_rows = passed_along(edge_rows, "ep", 1)
    values = conv_silu(tail_rows[:, :width_x], mixer_value_input, value_kernel)
    in_mat = conv_silu(
        tail_rows[:, width_x : width_x + width_b], input_state_matrix, input_matrix_kernel
    )
    out_mat = conv_silu(
        tail_rows[:, width_x + width_b :], output_state_matrix, output_matrix_kernel
    )
    step_length = jax.nn.softplus(step_input)
    decay_logarithm = -jnp.exp(head_log_decay)[None, :] * step_length + extra_log_decay
    running = jnp.cumsum(decay_logarithm.reshape(nblocks, BLOCK, heads_local), axis=1)
    value_wide = values.astype(jnp.float32).reshape(nblocks, BLOCK, heads_local, HEAD_DIM)
    scaled = value_wide * step_length.reshape(nblocks, BLOCK, heads_local)[..., None]
    in_blocks = in_mat.reshape(nblocks, BLOCK, groups_local, STATE)
    out_blocks = out_mat.reshape(nblocks, BLOCK, groups_local, STATE)
    scores = jnp.einsum(
        "bign,bjgn->bgij", out_blocks, in_blocks, preferred_element_type=jnp.float32
    )
    scores = jnp.repeat(scores, head_ratio, axis=1)
    spread = jnp.transpose(running[:, :, None, :] - running[:, None, :, :], (0, 3, 1, 2))
    lower_mask = jnp.tril(jnp.ones((BLOCK, BLOCK), bool))[None, None]
    decay_mat = jnp.where(lower_mask, jnp.exp(jnp.where(lower_mask, spread, 0.0)), 0.0)
    inside = jnp.einsum("bhij,bjhp->bihp", scores * decay_mat, scaled)
    out_head = jnp.repeat(out_blocks.astype(jnp.float32), head_ratio, axis=2)
    in_head = jnp.repeat(in_blocks.astype(jnp.float32), head_ratio, axis=2)
    block_logs = running[:, -1]
    to_end = jnp.exp(block_logs[:, None, :] - running)
    block_state = jnp.einsum("bjhn,bjh,bjhp->bhpn", in_head, to_end, scaled)
    start_state = jnp.zeros((heads_local, HEAD_DIM, STATE), jnp.float32)
    local_total, local_prev = lax.scan(
        carry_blocks, start_state, (jnp.exp(block_logs), block_state)
    )
    before_logs = jnp.cumsum(block_logs, axis=0) - block_logs
    incoming = carried_in(
        (jnp.exp(jnp.sum(block_logs, axis=0)), local_total),
        "ep",
        join_states,
        (jnp.ones((heads_local,), jnp.float32), start_state),
    )
    entering = local_prev + jnp.exp(before_logs)[:, :, None, None] * incoming[1][None]
    carried_term = jnp.einsum("bihn,bhpn->bihp", out_head, entering) * jnp.exp(running)[..., None]
    mixed_heads = (inside + carried_term).reshape(length, heads_local, HEAD_DIM)
    mixed_heads = mixed_heads + head_skip_scale[None, :, None] * value_wide.reshape(
        length, heads_local, HEAD_DIM
    )
    gated_heads = mixed_heads * jax.nn.silu(output_gate_input.astype(jnp.float32)).reshape(
        length, heads_local, HEAD_DIM
    )
    grouped = gated_heads.reshape(length, groups_local, head_ratio * HEAD_DIM)
    grouped = grouped * lax.rsqrt(jnp.mean(grouped * grouped, axis=-1, keepdims=True) + epsilon)
    mixer_normed = (grouped.reshape(length, width_x) * mixer_norm_scale).astype(jnp.bfloat16)
    rows_local = second_token_rows.shape[0]
    model_width = second_token_rows.shape[1]
    local_experts = routed_gate_weight.shape[0]
    ep_count = lax.axis_size("ep")
    experts = local_experts * ep_count
    capacity = max(2, 3 * rows_local * TOP_K // (2 * experts))
    col_width = model_width // lax.axis_size("tp")
    rows_wide = second_token_rows.astype(jnp.float32)
    normed = (
        rows_wide
        * lax.rsqrt(jnp.mean(rows_wide * rows_wide, axis=-1, keepdims=True) + epsilon)
        * expert_norm_scale
    ).astype(jnp.bfloat16)
    slot_owner, slot_index = route_slots(routed_expert_index, experts, capacity)
    padded = jnp.concatenate([normed, jnp.zeros((1, model_width), jnp.bfloat16)], axis=0)
    outgoing = jnp.take(padded, slot_owner, axis=0).reshape(experts, capacity, model_width)
    my_columns = lax.dynamic_slice_in_dim(outgoing, lax.axis_index("tp") * col_width, col_width, 2)
    arrived = lax.all_to_all(my_columns, "ep", split_axis=0, concat_axis=1, tiled=True)
    column_piece = lax.all_gather(arrived, "tp", axis=2, tiled=True)
    gate_pre = jnp.einsum(
        "esd,edf->esf", column_piece, routed_gate_weight, preferred_element_type=jnp.float32
    )
    up_pre = jnp.einsum(
        "esd,edf->esf", column_piece, routed_up_weight, preferred_element_type=jnp.float32
    )
    hidden = (jax.nn.silu(gate_pre) * up_pre).astype(jnp.bfloat16)
    shared_hidden = (
        jax.nn.silu(jnp.dot(normed, shared_gate_weight, preferred_element_type=jnp.float32))
        * jnp.dot(normed, shared_up_weight, preferred_element_type=jnp.float32)
    ).astype(jnp.bfloat16)
    whole_mix, whole_hidden, whole_shared = one_gather(
        (mixer_normed, hidden, shared_hidden), "tp", (1, 2, 1)
    )
    mixer_output = jnp.dot(
        whole_mix, mixer_output_weight, preferred_element_type=jnp.float32
    ).astype(jnp.bfloat16)
    expert_result = jnp.einsum(
        "esf,efd->esd", whole_hidden, routed_down_weight, preferred_element_type=jnp.float32
    ).astype(jnp.bfloat16)
    returned = lax.all_to_all(expert_result, "ep", split_axis=1, concat_axis=0, tiled=True)
    picked = jnp.take(returned.reshape(experts * capacity, col_width), slot_index, axis=0)
    picked = picked.reshape(rows_local, TOP_K, col_width).astype(jnp.float32)
    routed_sum = jnp.sum(picked * routed_expert_weight[:, :, None], axis=1)
    shared_result = jnp.dot(whole_shared, shared_down_weight, preferred_element_type=jnp.float32)
    routed_out = (routed_sum + shared_result).astype(jnp.bfloat16)
    return (mixer_output, routed_out)


def solution(mesh):
    return jax.shard_map(
        on_device,
        mesh=mesh,
        in_specs=(
            P("ep", "tp"),
            P("ep", "tp"),
            P("ep", "tp"),
            P("ep", "tp"),
            P("ep", "tp"),
            P("ep", "tp"),
            P("tp"),
            P("tp"),
            P(None, "tp"),
            P(None, "tp"),
            P(None, "tp"),
            P("tp"),
            P(None, "tp"),
            P("ep", None),
            P(),
            P("ep", None),
            P("ep", None),
            P("ep", None, "tp"),
            P("ep", None, "tp"),
            P("ep", None, "tp"),
            P(None, "tp"),
            P(None, "tp"),
            P(None, "tp"),
        ),
        out_specs=(P("ep", "tp"), P("ep", "tp")),
        check_vma=False,
    )
```

profile of v0, /device:TPU:1, one launch (start us, length us, event | category | flops | bytes accessed | tf_op | source)
XLA Modules:
  0.0 352.4 jit_solution(2182218224439034312)
XLA Ops:
  7.2 0.8 slice.100
  9.6 4.9 %collective-permute-start = (bf16[3,512]{0,1:T(8,128)(2,1)S(1)}, bf16[3,512]{0,1:T(8,128)(2,1)S(1)}, u32[]{:S(2)}, u32[]{:S(2)}) collective-permute-start(bf16[3,512]{0,1:T(8,128)(2,1)S(1)} %copy.125), channel_id=1, source_target_pairs={{0,16},{16,32},{32,48},{48,64},{64,80},{80,96},{96,112},{112,128},... | collective-permute-start | bytes 9224 | tf_op jit(solution)/shard_map/ppermute | solution.py:19
  15.2 0.8 compare_select_fusion.3
  17.6 0.8 slice_bitcast_fusion.3
  19.2 0.8 fusion.52
  20.6 0.8 copy.141
  21.6 1.0 copy.126
  23.7 0.8 broadcast_multiply_fusion
  25.8 18.0 %reduce-window.6 = s32[64,8,128]{2,1,0:T(8,128)S(1)} reduce-window(s32[64,8,128]{2,1,0:T(8,128)S(1)} %fusion.32, s32[]{:T(128)} %constant.114.clone.1), window={size=1x1x128 pad=0_0x0_0x127_0}, to_apply=%region_8.9 | reduce-window | flops 8323072 | bytes 524292 | tf_op jit(solution)/shard_map/reduce-window
  44.5 4.3 %scatter_custom_fusion = s32[1536]{0:T(1024)S(1)} fusion(s32[1024]{0:T(1024)S(1)} %bitcast.157, s32[1024]{0:T(1024)S(1)} %add_select_fusion, s32[]{:T(128)} %constant.119.clone.1), kind=kCustom, calls=%fused_computation.103 | custom fusion | bytes 6148 | tf_op jit(solution)/shard_map/scatter | solution.py:89
  49.8 1.5 fusion.3
  52.1 7.3 %gather_fusion = bf16[1536,2048]{1,0:T(8,128)(2,1)} fusion(bf16[257,2048]{1,0:T(8,128)(2,1)S(1)} %concatenate.22, s32[2048]{0:T(1024)} %pad_clamp_fusion), kind=kCustom, calls=%fused_computation | custom fusion | bytes 12589056 | tf_op jit(solution)/shard_map/jit(_take)/gather | solution.py:201
  59.5 1.3 dynamic-slice_select_fusion
  60.8 44.1 %all_to_all.33 = bf16[64,24,128]{2,1,0:T(8,128)(2,1)S(1)} all-to-all(bf16[64,24,128]{2,1,0:T(8,128)(2,1)S(1)} %dynamic-slice_select_fusion), channel_id=1, replica_groups=mesh['ep'=32,'tp'=16] {'ep'}, dimensions={0} | all-to-all | bytes 786432 | tf_op jit(solution)/shard_map/all_to_all | solution.py:203
  105.0 0.8 copy.145
  105.9 0.7 mul.357
  107.2 1.6 copy.131
  108.8 1.3 dynamic-slice
  111.6 46.4 %all-reduce.1 = bf16[128]{0:T(256)(128)(2,1)S(1)} all-reduce(bf16[128]{0:T(256)(128)(2,1)S(1)} %dynamic-update-slice), channel_id=2, replica_groups=mesh['ep'=32,'tp'=16] {'ep'}, use_global_device_ids=true, to_apply=%add.1 | all-reduce | flops 128 | bytes 512
  158.1 1.0 copy.138
  160.9 1.2 while.25
  160.9 1.0 convert_add_fusion.2
  162.1 1.3 fusion.5
  163.3 1.3 fusion.6
  165.4 21.0 %all-gather.7.cloned.1.call-done = bf16[2,768,2048]{2,1,0:T(8,128)(2,1)} async-done(((bf16[2,768,128]{2,1,0:T(8,128)(2,1)}), bf16[2,768,2048]{2,1,0:T(8,128)(2,1)}) %all-gather.7.cloned.1.call-update) | async-done | bytes 6291472 | tf_op jit(solution)/shard_map/all_gather | solution.py:204
  186.4 5.0 %fusion.54 = f32[2,768,64]{1,2,0:T(8,128)S(1)} fusion(bf16[2,768,2048]{2,1,0:T(8,128)(2,1)} %all-gather.7.cloned.1.call-done, bf16[2,2048,64]{1,2,0:T(8,128)(2,1)S(1)} %copy-done.5), kind=kOutput, calls=%fused_computation.129 | convolution fusion | flops 402653184 | bytes 7208960 | tf_op jit(solution)/shard_map/esd,edf->esf/dot_general | solution.py:205
  191.4 2.0 fusion.4
  193.8 0.8 pad_maximum_fusion
  194.6 74.8 %all-gather.11.cloned.1.call-done = bf16[2883584]{0:T(1024)(128)(2,1)} async-done(((bf16[180224]{0:T(1024)(128)(2,1)}), bf16[2883584]{0:T(1024)(128)(2,1)}) %all-gather.11.cloned.1.call-update) | async-done | bytes 5767184 | tf_op jit(solution)/shard_map/all_gather | solution.py:50
  269.4 5.8 %reshape.283 = bf16[16,180224]{1,0:T(8,128)(2,1)} reshape(bf16[2883584]{0:T(1024)(128)(2,1)} %all-gather.11.cloned.1.call-done) | data formatting | bytes 11534336 | tf_op jit(solution)/shard_map/all_gather | solution.py:50
  275.2 3.8 %slice.155 = bf16[16,98304]{1,0:T(8,128)(2,1)} slice(bf16[16,180224]{1,0:T(8,128)(2,1)} %reshape.283), slice={[0:16], [65536:163840]} | slice | bytes 6291456 | tf_op jit(solution)/shard_map/slice | solution.py:52
  279.0 8.8 %reshape.250 = bf16[16,2,768,64]{3,2,1,0:T(8,128)(2,1)} reshape(bf16[16,98304]{1,0:T(8,128)(2,1)} %slice.155) | data formatting | bytes 6291456 | tf_op jit(solution)/shard_map/reshape | solution.py:52
  287.8 6.9 %copy.151 = bf16[2,768,16,64]{1,3,2,0:T(8,128)(2,1)} copy(bf16[2,768,16,64]{3,1,0,2:T(8,128)(2,1)} %bitcast.128) | data formatting | bytes 6291456 | tf_op jit(solution)/shard_map/transpose | solution.py:43
  294.7 3.2 convolution_convert_fusion
  298.0 1.2 copy.153
  299.1 13.3 %all-to-all-start.1 = ((bf16[2,768,128]{2,0,1:T(2,128)(2,1)}), bf16[2,768,128]{2,0,1:T(2,128)(2,1)S(1)}, u32[]{:S(2)}, u32[]{:S(2)}) async-start(bf16[2,768,128]{2,0,1:T(2,128)(2,1)} %copy.153), calls=%async_computation.1 | async-start | bytes 786432 | tf_op jit(solution)/shard_map/all_to_all | solution.py:225
  312.6 0.8 copy.155
  313.5 0.8 copy.150
  314.3 3.1 slice.154
  317.4 1.1 reshape.253
  318.5 1.2 copy.156
  319.6 2.0 copy.162
  321.7 2.4 copy.148
  324.1 3.1 convolution_convert_fusion.1
  327.2 13.0 %all-to-all-done.1 = bf16[2,768,128]{2,0,1:T(2,128)(2,1)S(1)} async-done(((bf16[2,768,128]{2,0,1:T(2,128)(2,1)}), bf16[2,768,128]{2,0,1:T(2,128)(2,1)S(1)}, u32[]{:S(2)}, u32[]{:S(2)}) %all-to-all-start.1) | async-done | bytes 393248 | tf_op jit(solution)/shard_map/all_to_all | solution.py:225
  340.2 3.2 gather_fusion.1
  343.5 1.5 multiply_reduce_fusion
  344.9 1.0 fusion.7
  (138 shorter events, 15.0 us)
Async XLA Ops:
  7.2 317.0 %copy-start = (bf16[4096,128]{1,0:T(8,128)(2,1)S(1)}, bf16[4096,128]{1,0:T(8,128)(2,1)}, u32[]{:S(2)}) copy-start(bf16[4096,128]{1,0:T(8,128)(2,1)} %param.39) | copy-start | bytes 3145732
  7.2 17.3 %copy-start.14 = (bf16[256,128]{1,0:T(8,128)(2,1)S(1)}, bf16[256,128]{1,0:T(8,128)(2,1)}, u32[]{:S(2)}) copy-start(bf16[256,128]{1,0:T(8,128)(2,1)} %param.28) | copy-start | bytes 196612
  7.2 153.6 %all-gather.9.cloned.1.call-start = ((), (), s32[]{:S(2)}) async-start(), calls=%async_computation.3 | async-start | bytes 2162688 | tf_op jit(solution)/shard_map/all_gather | solution.py:25
  9.6 13.4 %collective-permute-start = (bf16[3,512]{0,1:T(8,128)(2,1)S(1)}, bf16[3,512]{0,1:T(8,128)(2,1)S(1)}, u32[]{:S(2)}, u32[]{:S(2)}) collective-permute-start(bf16[3,512]{0,1:T(8,128)(2,1)S(1)} %copy.125), channel_id=1, source_target_pairs={{0,16},{16,32},{32,48},{48,64},{64,80},{80,96},{96,112},{112,128},... | collective-permute-start | bytes 9224 | tf_op jit(solution)/shard_map/ppermute | solution.py:19
  16.3 5.3 %copy-start.4 = (f32[2,128,4]{2,1,0:T(8,128)}, f32[2,128,4]{2,1,0:T(8,128)S(1)}, u32[]{:S(2)}) copy-start(f32[2,128,4]{2,1,0:T(8,128)S(1)} %reduce_window_sum.37) | copy-start | bytes 12292
  24.8 24.8 %copy-start.2 = (bf16[256,2048]{1,0:T(8,128)(2,1)S(1)}, bf16[256,2048]{1,0:T(8,128)(2,1)}, u32[]{:S(2)}) copy-start(bf16[256,2048]{1,0:T(8,128)(2,1)} %param.40) | copy-start | bytes 3145732
  25.1 0.7 copy-start.9
  25.8 160.6 %all-gather.7.cloned.1.call-start = ((), (), s32[]{:S(2)}) async-start(), calls=%async_computation.2 | async-start | bytes 6684672 | tf_op jit(solution)/shard_map/all_gather | solution.py:204
  52.1 7.4 %copy-start.17 = (pred[64,24]{1,0:T(8,128)(4,1)S(1)}, pred[64,24]{1,0:T(8,128)(4,1)}, u32[]{:S(2)}) copy-start(pred[64,24]{1,0:T(8,128)(4,1)} %broadcast_in_dim.85) | copy-start | bytes 4612
  59.5 99.7 %copy-start.6 = (f32[2,128,4]{2,1,0:T(8,128)S(1)}, f32[2,128,4]{2,1,0:T(8,128)}, u32[]{:S(2)}) copy-start(f32[2,128,4]{2,1,0:T(8,128)} %get-tuple-element.121) | copy-start | bytes 12292
  59.5 99.8 %copy-start.10 = (bf16[2048,64]{0,1:T(8,128)(2,1)S(1)}, bf16[2048,64]{0,1:T(8,128)(2,1)}, u32[]{:S(2)}) copy-start(bf16[2048,64]{0,1:T(8,128)(2,1)} %param.47) | copy-start | bytes 786436
  59.5 100.2 %copy-start.11 = (bf16[2048,64]{0,1:T(8,128)(2,1)S(1)}, bf16[2048,64]{0,1:T(8,128)(2,1)}, u32[]{:S(2)}) copy-start(bf16[2048,64]{0,1:T(8,128)(2,1)} %param.48) | copy-start | bytes 786436
  59.5 100.9 %copy-start.20 = (f32[4,128]{1,0:T(4,128)S(1)}, f32[4,128]{1,0:T(4,128)}, u32[]{:S(2)}) copy-start(f32[4,128]{1,0:T(4,128)} %param.37) | copy-start | bytes 6148
  59.5 101.0 %copy-start.15 = (bf16[256,128]{1,0:T(8,128)(2,1)S(1)}, bf16[256,128]{1,0:T(8,128)(2,1)}, u32[]{:S(2)}) copy-start(bf16[256,128]{1,0:T(8,128)(2,1)} %param.29) | copy-start | bytes 196612
  105.8 163.6 %all-gather.11.cloned.1.call-start = ((), (), s32[]{:S(2)}) async-start(), calls=%async_computation.4 | async-start | bytes 6127616 | tf_op jit(solution)/shard_map/all_gather | solution.py:50
  160.1 4.7 %copy-start.18 = (f32[256]{0:T(256)S(1)}, f32[256]{0:T(256)}, u32[]{:S(2)}) copy-start(f32[256]{0:T(256)} %mul.358) | copy-start | bytes 3076
  160.1 4.9 %copy-start.21 = (f32[256]{0:T(256)S(1)}, f32[256]{0:T(256)}, u32[]{:S(2)}) copy-start(f32[256]{0:T(256)} %param.38) | copy-start | bytes 3076
  160.8 25.6 %copy-start.5 = (bf16[2,2048,64]{1,2,0:T(8,128)(2,1)S(1)}, bf16[2,2048,64]{1,2,0:T(8,128)(2,1)}, u32[]{:S(2)}) copy-start(bf16[2,2048,64]{1,2,0:T(8,128)(2,1)} %param.44) | copy-start | bytes 1572868
  165.4 26.0 %copy-start.22 = (bf16[2,2048,64]{1,2,0:T(8,128)(2,1)S(1)}, bf16[2,2048,64]{1,2,0:T(8,128)(2,1)}, u32[]{:S(2)}) copy-start(bf16[2,2048,64]{1,2,0:T(8,128)(2,1)} %param.45) | copy-start | bytes 1572868
  186.4 5.0 %copy-start.1 = (bf16[2,768,2048]{2,1,0:T(8,128)(2,1)S(1)}, bf16[2,768,2048]{2,1,0:T(8,128)(2,1)}, u32[]{:S(2)}) copy-start(bf16[2,768,2048]{2,1,0:T(8,128)(2,1)} %all-gather.7.cloned.1.call-done) | copy-start | bytes 18874372
  287.8 6.9 %copy-start.8 = (bf16[2,1024,128]{2,1,0:T(8,128)(2,1)S(1)}, bf16[2,1024,128]{2,1,0:T(8,128)(2,1)}, u32[]{:S(2)}) copy-start(bf16[2,1024,128]{2,1,0:T(8,128)(2,1)} %param.46) | copy-start | bytes 1572868
  294.7 17.9 %copy-start.19 = (f32[256,4]{0,1:T(4,128)S(1)}, f32[256,4]{0,1:T(4,128)}, u32[]{:S(2)}) copy-start(f32[256,4]{0,1:T(4,128)} %param.43) | copy-start | bytes 12292
  294.7 18.8 %copy-start.16 = (s32[256,4]{0,1:T(4,128)S(1)}, s32[256,4]{0,1:T(4,128)}, u32[]{:S(2)}) copy-start(s32[256,4]{0,1:T(4,128)} %param.42) | copy-start | bytes 12292
  299.1 18.2 %slice-start = ((bf16[16,180224]{1,0:T(8,128)(2,1)}), bf16[16,16384]{1,0:T(8,128)(2,1)S(1)}, s32[]{:S(2)}) async-start(bf16[16,180224]{1,0:T(8,128)(2,1)} %reshape.283), calls=%async_computation.5 | async-start | bytes 1048576 | tf_op jit(solution)/shard_map/slice | solution.py:52
  299.1 41.0 %all-to-all-start.1 = ((bf16[2,768,128]{2,0,1:T(2,128)(2,1)}), bf16[2,768,128]{2,0,1:T(2,128)(2,1)S(1)}, u32[]{:S(2)}, u32[]{:S(2)}) async-start(bf16[2,768,128]{2,0,1:T(2,128)(2,1)} %copy.153), calls=%async_computation.1 | async-start | bytes 786432 | tf_op jit(solution)/shard_map/all_to_all | solution.py:225
  324.1 19.3 %copy-start.7 = (f32[256,4]{1,0:T(8,128)S(1)}, f32[256,4]{1,0:T(8,128)}, u32[]{:S(2)}) copy-start(f32[256,4]{1,0:T(8,128)} %copy.155) | copy-start | bytes 12292
  324.1 19.3 %copy-start.13 = (pred[256,4]{1,0:T(8,128)(4,1)S(1)}, pred[256,4]{1,0:T(8,128)(4,1)}, u32[]{:S(2)}) copy-start(pred[256,4]{1,0:T(8,128)(4,1)} %copy.150) | copy-start | bytes 3076
  324.1 20.8 %copy-start.3 = (bf16[256,16,64]{0,2,1:T(8,128)(2,1)S(1)}, bf16[256,16,64]{0,2,1:T(8,128)(2,1)}, u32[]{:S(2)}) copy-start(bf16[256,16,64]{0,2,1:T(8,128)(2,1)} %copy.156) | copy-start | bytes 1572868
  324.1 20.8 %copy-start.12 = (bf16[1024,128]{1,0:T(8,128)(2,1)S(1)}, bf16[1024,128]{1,0:T(8,128)(2,1)}, u32[]{:S(2)}) copy-start(bf16[1024,128]{1,0:T(8,128)(2,1)} %param.49) | copy-start | bytes 786436
Sparse Core Ops, SparseCore 0:
  25.9 80.0 all-gather.8
  108.9 77.3 all-gather.6
  194.7 74.6 all-gather.10
where the time goes:
time: 355 us; the launch traced here: 352 us
  waiting for transfers between devices  109 us (31%)
  blocking collectives  90.6 us (26%)
  local copies, waits for them, and re-layouts  68.7 us (19%)
  other arithmetic  32.7 us (9%)
  starting transfers between devices  18.3 us (5%)
  matrix products  18.1 us (5%)
  between operations  15 us (4%)
    all_gather x1, waiting for transfers between devices, one_gather(): lines, at, finished = (lax.all_gather(ravelled, axis), 0, [])  74.8 us
    unnamed x1, blocking collectives  46.4 us
    all_to_all x1, blocking collectives, on_device(): lax.all_to_all(my_columns, 'ep', split_axis=0, concat_axis=1, tiled=True)  44.1 us
    all_gather x1, waiting for transfers between devices, on_device(): column_piece = lax.all_gather(arrived, 'tp', axis=2, tiled=True)  21 us
    another operation x3, other arithmetic  18.2 us
    all_to_all x1, starting transfers between devices, on_device(): lax.all_to_all(expert_result, 'ep', split_axis=1, concat_axis=0, tiled=True)  13.3 us
    all_to_all x1, waiting for transfers between devices, on_device(): lax.all_to_all(expert_result, 'ep', split_axis=1, concat_axis=0, tiled=True)  13 us
    transpose x3, local copies, waits for them, and re-layouts, laid_out(): tiles = jnp.moveaxis(tiles, 0, dim)  10.5 us
  transfers between devices with their start and end apart: 5, of which 3 were waited for; matrix products, arithmetic and copies ran while one was open for 20% of the time, Pallas kernels for 0%

commit v1 on v0

v1 whole, which is shorter than its diff:
```python
import jax
import jax.numpy as jnp
from jax import lax
from jax.sharding import PartitionSpec as P

HEAD_DIM = 64
STATE = 128
CONV_TAPS = 4
BLOCK = 128
TOP_K = 4
epsilon = 1e-05
F32 = jnp.float32
BF16 = jnp.bfloat16


def passed_along(x, axis, by):
    size = lax.axis_size(axis)
    pairs = [(i, i + by) for i in range(size) if 0 <= i + by < size]
    return lax.ppermute(x, axis, pairs)


def high(x):
    return lax.reduce_precision(x, 8, 7)


def three_parts(x):
    a = high(x)
    b = high(x - a)
    return a, b, x - a - b


def laid_out(tiles, dim):
    tiles = jnp.moveaxis(tiles, 0, dim)
    dims = tiles.shape
    return tiles.reshape(*dims[:dim], dims[dim] * dims[dim + 1], *dims[dim + 2 :])


def one_gather(arrays, axis, dims):
    ravelled = jnp.concatenate([a.reshape(-1) for a in arrays])
    lines, at, finished = (lax.all_gather(ravelled, axis), 0, [])
    for a, dim in zip(arrays, dims):
        tiles = lines[:, at : at + a.size].reshape(-1, *a.shape)
        finished.append(laid_out(tiles, dim))
        at += a.size
    return tuple(finished)


def conv_silu(tail_rows, source, weights):
    length = source.shape[0]
    padded = jnp.concatenate([tail_rows, source], axis=0)
    total_sum = jnp.zeros(source.shape, F32)
    for tap_index in range(CONV_TAPS):
        total_sum = (
            total_sum
            + padded[tap_index : tap_index + length].astype(F32) * weights[tap_index]
        )
    return jax.nn.silu(total_sum).astype(BF16)


def state_before(log_total, total_state):
    heads = log_total.shape[0]
    count = lax.axis_size("ep")
    place = lax.axis_index("ep")
    parts = jnp.stack(three_parts(log_total)).reshape(1, 3 * heads)
    row = jnp.pad(parts, ((0, 15), (0, STATE - 3 * heads)))
    rows = heads * HEAD_DIM
    payload = jnp.concatenate([total_state.reshape(rows, STATE), row], axis=0).astype(BF16)
    gathered = lax.all_gather(payload, "ep")
    tail = gathered[:, rows, : 3 * heads].astype(F32).reshape(count, 3, heads)
    logs = jnp.sum(tail, axis=1)
    at = jnp.arange(count)
    between = (at[None, :] > at[:, None]) & (at[None, :] < place)
    spans = jnp.sum(jnp.where(between[:, :, None], logs[None], 0.0), axis=1)
    weights = jnp.where((at < place)[:, None], jnp.exp(spans), 0.0)
    wide = jnp.repeat(weights, HEAD_DIM, axis=1)[:, :, None]
    summed = jnp.sum(gathered[:, :rows, :].astype(F32) * wide, axis=0)
    return summed.reshape(heads, HEAD_DIM, STATE)


def routes(index_t, weight_t, experts, capacity):
    rows = index_t.shape[1]
    ids = jnp.arange(experts, dtype=jnp.int32)[:, None]
    named = jnp.zeros((experts, rows), F32)
    weight = jnp.zeros((experts, rows), F32)
    for k in range(TOP_K):
        hit = index_t[k][None, :] == ids
        named = jnp.where(hit, 1.0, named)
        weight = jnp.where(hit, weight_t[k][None, :], weight)
    at = jnp.arange(rows)
    earlier = (at[:, None] < at[None, :]).astype(BF16)
    place = jnp.dot(named.astype(BF16), earlier, preferred_element_type=F32)
    place = jnp.where(named > 0.0, place, -1.0)
    slots = jnp.arange(capacity, dtype=jnp.int32).astype(F32)[None, :, None]
    taken = place[:, None, :] == slots
    return taken, weight


def on_device(
    mixer_value_input,
    input_state_matrix,
    output_state_matrix,
    output_gate_input,
    step_input,
    extra_log_decay,
    head_log_decay,
    head_skip_scale,
    value_kernel,
    input_matrix_kernel,
    output_matrix_kernel,
    mixer_norm_scale,
    mixer_output_weight,
    second_token_rows,
    expert_norm_scale,
    routed_expert_index,
    routed_expert_weight,
    routed_gate_weight,
    routed_up_weight,
    routed_down_weight,
    shared_gate_weight,
    shared_up_weight,
    shared_down_weight,
):
    length = mixer_value_input.shape[0]
    heads_local = step_input.shape[1]
    width_x = mixer_value_input.shape[1]
    width_b = input_state_matrix.shape[1]
    groups_local = width_b // STATE
    head_ratio = heads_local // groups_local
    nblocks = length // BLOCK
    lead_row = length - CONV_TAPS + 1
    edge_rows = jnp.concatenate(
        [
            mixer_value_input[lead_row:],
            input_state_matrix[lead_row:],
            output_state_matrix[lead_row:],
        ],
        axis=1,
    )
    tail_rows = passed_along(edge_rows, "ep", 1)
    values = conv_silu(tail_rows[:, :width_x], mixer_value_input, value_kernel)
    in_mat = conv_silu(
        tail_rows[:, width_x : width_x + width_b], input_state_matrix, input_matrix_kernel
    )
    out_mat = conv_silu(
        tail_rows[:, width_x + width_b :], output_state_matrix, output_matrix_kernel
    )
    step_length = jax.nn.softplus(step_input)
    decay_logarithm = -jnp.exp(head_log_decay)[None, :] * step_length + extra_log_decay
    running = jnp.cumsum(decay_logarithm.reshape(nblocks, BLOCK, heads_local), axis=1)
    value_wide = values.astype(F32).reshape(nblocks, BLOCK, heads_local, HEAD_DIM)
    scaled = value_wide * step_length.reshape(nblocks, BLOCK, heads_local)[..., None]
    in_blocks = in_mat.reshape(nblocks, BLOCK, groups_local, STATE)
    out_blocks = out_mat.reshape(nblocks, BLOCK, groups_local, STATE)
    scores = jnp.einsum("bign,bjgn->bgij", out_blocks, in_blocks, preferred_element_type=F32)
    scores = jnp.repeat(scores, head_ratio, axis=1)
    spread = jnp.transpose(running[:, :, None, :] - running[:, None, :, :], (0, 3, 1, 2))
    lower_mask = jnp.tril(jnp.ones((BLOCK, BLOCK), bool))[None, None]
    decay_mat = jnp.where(lower_mask, jnp.exp(jnp.where(lower_mask, spread, 0.0)), 0.0)
    inside = jnp.einsum("bhij,bjhp->bihp", scores * decay_mat, scaled)
    out_head = jnp.repeat(out_blocks.astype(F32), head_ratio, axis=2)
    in_head = jnp.repeat(in_blocks.astype(F32), head_ratio, axis=2)
    block_logs = running[:, -1]
    to_end = jnp.exp(block_logs[:, None, :] - running)
    block_state = jnp.einsum("bjhn,bjh,bjhp->bhpn", in_head, to_end, scaled)
    carried = jnp.zeros((heads_local, HEAD_DIM, STATE), F32)
    before = []
    for b in range(nblocks):
        before.append(carried)
        carried = carried * jnp.exp(block_logs[b])[:, None, None] + block_state[b]
    local_prev = jnp.stack(before)
    before_logs = jnp.cumsum(block_logs, axis=0) - block_logs
    incoming = state_before(jnp.sum(block_logs, axis=0), carried)
    entering = local_prev + jnp.exp(before_logs)[:, :, None, None] * incoming[None]
    carried_term = jnp.einsum("bihn,bhpn->bihp", out_head, entering) * jnp.exp(running)[..., None]
    mixed_heads = (inside + carried_term).reshape(length, heads_local, HEAD_DIM)
    mixed_heads = mixed_heads + head_skip_scale[None, :, None] * value_wide.reshape(
        length, heads_local, HEAD_DIM
    )
    gated_heads = mixed_heads * jax.nn.silu(output_gate_input.astype(F32)).reshape(
        length, heads_local, HEAD_DIM
    )
    grouped = gated_heads.reshape(length, groups_local, head_ratio * HEAD_DIM)
    grouped = grouped * lax.rsqrt(jnp.mean(grouped * grouped, axis=-1, keepdims=True) + epsilon)
    mixer_normed = (grouped.reshape(length, width_x) * mixer_norm_scale).astype(BF16)

    rows_local = second_token_rows.shape[0]
    model_width = second_token_rows.shape[1]
    local_experts = routed_gate_weight.shape[0]
    ep_count = lax.axis_size("ep")
    experts = local_experts * ep_count
    capacity = max(2, 3 * rows_local * TOP_K // (2 * experts))
    col_width = model_width // lax.axis_size("tp")
    rows_wide = second_token_rows.astype(F32)
    normed = (
        rows_wide
        * lax.rsqrt(jnp.mean(rows_wide * rows_wide, axis=-1, keepdims=True) + epsilon)
        * expert_norm_scale
    ).astype(BF16)
    taken, weight = routes(routed_expert_index.T, routed_expert_weight.T, experts, capacity)
    one_hot = taken.astype(BF16).reshape(experts * capacity, rows_local)
    mine = lax.dynamic_slice_in_dim(normed, lax.axis_index("tp") * col_width, col_width, 1)
    my_columns = jnp.dot(one_hot, mine, preferred_element_type=F32).astype(BF16)
    my_columns = my_columns.reshape(experts, capacity, col_width)
    arrived = lax.all_to_all(my_columns, "ep", split_axis=0, concat_axis=1, tiled=True)
    column_piece = lax.all_gather(arrived, "tp", axis=2, tiled=True)
    gate_pre = jnp.einsum(
        "esd,edf->esf", column_piece, routed_gate_weight, preferred_element_type=F32
    )
    up_pre = jnp.einsum("esd,edf->esf", column_piece, routed_up_weight, preferred_element_type=F32)
    hidden = (jax.nn.silu(gate_pre) * up_pre).astype(BF16)
    shared_hidden = (
        jax.nn.silu(jnp.dot(normed, shared_gate_weight, preferred_element_type=F32))
        * jnp.dot(normed, shared_up_weight, preferred_element_type=F32)
    ).astype(BF16)
    whole_mix, whole_hidden, whole_shared = one_gather(
        (mixer_normed, hidden, shared_hidden), "tp", (1, 2, 1)
    )
    mixer_output = jnp.dot(whole_mix, mixer_output_weight, preferred_element_type=F32).astype(BF16)
    expert_result = jnp.einsum(
        "esf,efd->esd", whole_hidden, routed_down_weight, preferred_element_type=F32
    ).astype(BF16)
    returned = lax.all_to_all(expert_result, "ep", split_axis=1, concat_axis=0, tiled=True)
    returned = returned.reshape(experts * capacity, col_width)
    weight_high = high(weight)
    contract = (((0,), (0,)), ((), ()))
    routed_sum = jnp.zeros((rows_local, col_width), F32)
    for part in (weight_high, weight - weight_high):
        spread_part = jnp.where(taken, part[:, None, :], 0.0).astype(BF16)
        spread_part = spread_part.reshape(experts * capacity, rows_local)
        routed_sum = routed_sum + lax.dot_general(
            spread_part, returned, contract, preferred_element_type=F32
        )
    shared_result = jnp.dot(whole_shared, shared_down_weight, preferred_element_type=F32)
    routed_out = (routed_sum + shared_result).astype(BF16)
    return (mixer_output, routed_out)


def solution(mesh):
    return jax.shard_map(
        on_device,
        mesh=mesh,
        in_specs=(
            P("ep", "tp"),
            P("ep", "tp"),
            P("ep", "tp"),
            P("ep", "tp"),
            P("ep", "tp"),
            P("ep", "tp"),
            P("tp"),
            P("tp"),
            P(None, "tp"),
            P(None, "tp"),
            P(None, "tp"),
            P("tp"),
            P(None, "tp"),
            P("ep", None),
            P(),
            P("ep", None),
            P("ep", None),
            P("ep", None, "tp"),
            P("ep", None, "tp"),
            P("ep", None, "tp"),
            P(None, "tp"),
            P(None, "tp"),
            P(None, "tp"),
        ),
        out_specs=(P("ep", "tp"), P("ep", "tp")),
        check_vma=False,
    )
```

time: 355 us -> 347 us (0.977)
  waiting for transfers between devices: 109 us -> 190 us
  blocking collectives: 90.6 us -> 44.8 us
  local copies, waits for them, and re-layouts: 68.7 us -> 46.7 us
  other arithmetic: 32.7 us -> 12.5 us
    all_gather x1, waiting for transfers between devices: 21 us -> 73.3 us  [on_device(): column_piece = lax.all_gather(arrived, 'tp', axis=2, tiled=True)]
    unnamed x1 -> x0, blocking collectives: 46.4 us -> none
    all_gather x1, waiting for transfers between devices: 0.02 us -> 28.7 us  [state_before(): gathered = lax.all_gather(payload, 'ep')]
    another operation x3, other arithmetic: 18.2 us -> 0.15 us
    gather x2 -> x0, local copies, waits for them, and re-layouts: 10.6 us -> none  [the longest x1 7.34 us: on_device(): jnp.take(padded, slot_owner, axis=0).reshape(experts, capacity, model_width)]
    scatter x1 -> x0, local copies, waits for them, and re-layouts: 4.32 us -> none  [route_slots(): slot_owner = jnp.full((experts * capacity,), route_block.shape[0], jnp.in...]
    unnamed x55 -> x75, local copies, waits for them, and re-layouts: 7.44 us -> 3.53 us
    dot_general x4 -> x8, matrix products: 4.93 us -> 8.24 us  [the longest x1 3.05 us: on_device(): jnp.dot(whole_mix, mixer_output_weight, preferred_element_type=F32)]
  transfers between devices with their start and end apart: 5 -> 5, of which waited for: 3 -> 4; matrix products, arithmetic and copies ran while one was open for 20% -> 9% of each run, Pallas kernels for 0% -> 0%
where the time goes in v1:
time: 347 us; the launch traced here: 346 us
  waiting for transfers between devices  190 us (55%)
  local copies, waits for them, and re-layouts  46.7 us (13%)
  blocking collectives  44.8 us (13%)
  matrix products  19.5 us (6%)
  starting transfers between devices  18.2 us (5%)
  between operations  14.5 us (4%)
  other arithmetic  12.5 us (4%)
    all_gather x1, waiting for transfers between devices, one_gather(): lines, at, finished = (lax.all_gather(ravelled, axis), 0, [])  74.8 us
    all_gather x1, waiting for transfers between devices, on_device(): column_piece = lax.all_gather(arrived, 'tp', axis=2, tiled=True)  73.3 us
    all_to_all x1, blocking collectives, on_device(): lax.all_to_all(my_columns, 'ep', split_axis=0, concat_axis=1, tiled=True)  44.8 us
    all_gather x1, waiting for transfers between devices, state_before(): gathered = lax.all_gather(payload, 'ep')  28.7 us
    all_to_all x1, starting transfers between devices, on_device(): lax.all_to_all(expert_result, 'ep', split_axis=1, concat_axis=0, tiled=True)  13.2 us
    all_to_all x1, waiting for transfers between devices, on_device(): lax.all_to_all(expert_result, 'ep', split_axis=1, concat_axis=0, tiled=True)  12.9 us
    transpose x3, local copies, waits for them, and re-layouts, laid_out(): tiles = jnp.moveaxis(tiles, 0, dim)  10.4 us
    reshape x2, local copies, waits for them, and re-layouts, one_gather(): tiles = lines[:, at:at + a.size].reshape(-1, *a.shape)  9.96 us
  transfers between devices with their start and end apart: 5, of which 4 were waited for; matrix products, arithmetic and copies ran while one was open for 9% of the time, Pallas kernels for 0%

profile of v1, /device:TPU:1, one launch (start us, length us, event | category | flops | bytes accessed | tf_op | source)
XLA Modules:
  0.0 346.0 jit_solution(6306174903025940382)
XLA Ops:
  7.2 0.8 slice.140
  8.0 0.7 slice.141
  8.7 0.7 slice.139
  9.6 4.9 %collective-permute-start = (bf16[3,512]{0,1:T(8,128)(2,1)S(1)}, bf16[3,512]{0,1:T(8,128)(2,1)S(1)}, u32[]{:S(2)}, u32[]{:S(2)}) collective-permute-start(bf16[3,512]{0,1:T(8,128)(2,1)S(1)} %copy.162), channel_id=1, source_target_pairs={{0,16},{16,32},{32,48},{48,64},{64,80},{80,96},{96,112},{112,128},... | collective-permute-start | bytes 9224 | tf_op jit(solution)/shard_map/ppermute | solution.py:19
  14.5 0.7 exponential_negate_fusion
  15.2 0.8 compare_select_fusion.2
  16.3 0.8 slice_bitcast_fusion.3
  17.2 0.8 fusion.70
  18.1 0.7 fusion.67
  18.8 1.0 copy.163
  20.2 0.6 fusion.68
  21.0 0.4 fusion.38
  21.5 0.8 broadcast_multiply_fusion
  22.6 0.8 fusion.66
  23.5 0.6 pad_maximum_fusion.2
  25.6 0.4 convolution_convert_fusion
  26.0 44.8 %all_to_all.33 = bf16[64,24,128]{2,1,0:T(8,128)(2,1)S(1)} all-to-all(bf16[64,24,128]{2,1,0:T(8,128)(2,1)S(1)} %bitcast.139), channel_id=1, replica_groups=mesh['ep'=32,'tp'=16] {'ep'}, dimensions={0} | all-to-all | bytes 786432 | tf_op jit(solution)/shard_map/all_to_all | solution.py:204
  70.8 0.8 copy.179
  72.1 1.4 fusion.74
  73.6 1.4 fusion.9
  75.7 28.7 %all-gather.5.cloned.1.call-done = bf16[32,272,128]{2,1,0:T(8,128)(2,1)} async-done(((bf16[1,272,128]{2,1,0:T(8,128)(2,1)}), bf16[32,272,128]{2,1,0:T(8,128)(2,1)}) %all-gather.5.cloned.1.call-update) | async-done | bytes 2228240 | tf_op jit(solution)/shard_map/all_gather | solution.py:68
  104.4 0.8 slice.205
  105.8 3.3 multiply_reduce_fusion
  109.1 0.3 fusion.6
  109.5 0.4 fusion.7
  110.6 73.3 %all-gather.7.cloned.1.call-done = bf16[2,768,2048]{2,1,0:T(8,128)(2,1)} async-done(((bf16[2,768,128]{2,1,0:T(8,128)(2,1)}), bf16[2,768,2048]{2,1,0:T(8,128)(2,1)}) %all-gather.7.cloned.1.call-update) | async-done | bytes 6291472 | tf_op jit(solution)/shard_map/all_gather | solution.py:205
  183.9 5.0 %fusion.73 = f32[2,768,64]{1,2,0:T(8,128)S(1)} fusion(bf16[2,768,2048]{2,1,0:T(8,128)(2,1)} %all-gather.7.cloned.1.call-done, bf16[2,2048,64]{1,2,0:T(8,128)(2,1)S(1)} %copy-done.8), kind=kOutput, calls=%fused_computation.151 | convolution fusion | flops 402653184 | bytes 7208960 | tf_op jit(solution)/shard_map/esd,edf->esf/dot_general | solution.py:206
  188.9 2.0 fusion.5
  191.3 0.8 pad_maximum_fusion
  192.1 74.8 %all-gather.9.cloned.1.call-done = bf16[2883584]{0:T(1024)(128)(2,1)} async-done(((bf16[180224]{0:T(1024)(128)(2,1)}), bf16[2883584]{0:T(1024)(128)(2,1)}) %all-gather.9.cloned.1.call-update) | async-done | bytes 5767184 | tf_op jit(solution)/shard_map/all_gather | solution.py:40
  266.9 5.8 %reshape.648 = bf16[16,180224]{1,0:T(8,128)(2,1)} reshape(bf16[2883584]{0:T(1024)(128)(2,1)} %all-gather.9.cloned.1.call-done) | data formatting | bytes 11534336 | tf_op jit(solution)/shard_map/all_gather | solution.py:40
  272.7 3.7 %slice.215 = bf16[16,98304]{1,0:T(8,128)(2,1)} slice(bf16[16,180224]{1,0:T(8,128)(2,1)} %reshape.648), slice={[0:16], [65536:163840]} | slice | bytes 6291456 | tf_op jit(solution)/shard_map/slice | solution.py:42
  276.4 8.8 %reshape.642 = bf16[16,2,768,64]{3,2,1,0:T(8,128)(2,1)} reshape(bf16[16,98304]{1,0:T(8,128)(2,1)} %slice.215) | data formatting | bytes 6291456 | tf_op jit(solution)/shard_map/reshape | solution.py:42
  285.3 6.9 %copy.183 = bf16[2,768,16,64]{1,3,2,0:T(8,128)(2,1)} copy(bf16[2,768,16,64]{3,1,0,2:T(8,128)(2,1)} %bitcast.127) | data formatting | bytes 6291456 | tf_op jit(solution)/shard_map/transpose | solution.py:33
  292.2 3.3 convolution_convert_fusion.1
  295.5 1.2 copy.185
  296.6 13.2 %all-to-all-start.1 = ((bf16[2,768,128]{2,0,1:T(2,128)(2,1)}), bf16[2,768,128]{2,0,1:T(2,128)(2,1)S(1)}, u32[]{:S(2)}, u32[]{:S(2)}) async-start(bf16[2,768,128]{2,0,1:T(2,128)(2,1)} %copy.185), calls=%async_computation.1 | async-start | bytes 786432 | tf_op jit(solution)/shard_map/all_to_all | solution.py:222
  309.9 1.8 fusion.4
  311.7 3.1 slice.210
  314.8 1.1 reshape.645
  316.0 1.1 copy.188
  317.1 2.0 copy.194
  319.2 2.4 copy.182
  321.6 3.0 convolution_convert_fusion.2
  324.6 12.9 %all-to-all-done.1 = bf16[2,768,128]{2,0,1:T(2,128)(2,1)S(1)} async-done(((bf16[2,768,128]{2,0,1:T(2,128)(2,1)}), bf16[2,768,128]{2,0,1:T(2,128)(2,1)S(1)}, u32[]{:S(2)}, u32[]{:S(2)}) %all-to-all-start.1) | async-done | bytes 393248 | tf_op jit(solution)/shard_map/all_to_all | solution.py:222
  337.7 0.4 fusion.75
  338.1 0.4 convolution_add_fusion.1
  338.5 1.0 fusion.8
  (146 shorter events, 6.0 us)
Async XLA Ops:
  7.2 314.4 %copy-start = (bf16[4096,128]{1,0:T(8,128)(2,1)S(1)}, bf16[4096,128]{1,0:T(8,128)(2,1)}, u32[]{:S(2)}) copy-start(bf16[4096,128]{1,0:T(8,128)(2,1)} %param.35) | copy-start | bytes 3145732
  7.2 15.1 %copy-start.18 = (bf16[256,128]{1,0:T(8,128)(2,1)S(1)}, bf16[256,128]{1,0:T(8,128)(2,1)}, u32[]{:S(2)}) copy-start(bf16[256,128]{1,0:T(8,128)(2,1)} %param.24) | copy-start | bytes 196612
  7.2 97.2 %all-gather.5.cloned.1.call-start = ((), (), s32[]{:S(2)}) async-start(), calls=%async_computation.2 | async-start | bytes 2297856 | tf_op jit(solution)/shard_map/all_gather | solution.py:68
  9.6 10.7 %collective-permute-start = (bf16[3,512]{0,1:T(8,128)(2,1)S(1)}, bf16[3,512]{0,1:T(8,128)(2,1)S(1)}, u32[]{:S(2)}, u32[]{:S(2)}) collective-permute-start(bf16[3,512]{0,1:T(8,128)(2,1)S(1)} %copy.162), channel_id=1, source_target_pairs={{0,16},{16,32},{32,48},{48,64},{64,80},{80,96},{96,112},{112,128},... | collective-permute-start | bytes 9224 | tf_op jit(solution)/shard_map/ppermute | solution.py:19
  18.1 6.2 %copy-start.27 = (s32[256,4]{0,1:T(4,128)S(1)}, s32[256,4]{0,1:T(4,128)}, u32[]{:S(2)}) copy-start(s32[256,4]{0,1:T(4,128)} %param.38) | copy-start | bytes 12292
  20.9 3.9 %copy-start.2 = (bf16[256,2048]{1,0:T(8,128)(2,1)S(1)}, bf16[256,2048]{1,0:T(8,128)(2,1)}, u32[]{:S(2)}) copy-start(bf16[256,2048]{1,0:T(8,128)(2,1)} %param.36) | copy-start | bytes 3145732
  21.5 3.7 %copy-start.20 = (f32[2048]{0:T(1024)S(1)}, f32[2048]{0:T(1024)}, u32[]{:S(2)}) copy-start(f32[2048]{0:T(1024)} %param.37) | copy-start | bytes 24580
  22.4 1.0 copy-start.6
  24.2 159.7 %all-gather.7.cloned.1.call-start = ((), (), s32[]{:S(2)}) async-start(), calls=%async_computation.3 | async-start | bytes 6684672 | tf_op jit(solution)/shard_map/all_gather | solution.py:205
  24.2 0.9 copy-start.29
  24.4 0.8 copy-start.21
  24.4 0.8 copy-start.23
  24.4 0.8 copy-start.25
  24.6 0.6 copy-start.12
  25.5 46.2 %copy-start.33 = (f32[4]{0:T(128)S(1)}, f32[4]{0:T(128)}, u32[]{:S(2)}) copy-start(f32[4]{0:T(128)} %param.30) | copy-start | bytes 52
  25.6 46.4 %copy-start.15 = (bf16[256,256]{1,0:T(8,128)(2,1)S(1)}, bf16[256,256]{1,0:T(8,128)(2,1)}, u32[]{:S(2)}) copy-start(bf16[256,256]{1,0:T(8,128)(2,1)} %param.26) | copy-start | bytes 393220
  25.6 46.5 %copy-start.9 = (f32[2,128,4]{2,1,0:T(8,128)S(1)}, f32[2,128,4]{2,1,0:T(8,128)}, u32[]{:S(2)}) copy-start(f32[2,128,4]{2,1,0:T(8,128)} %get-tuple-element.13) | copy-start | bytes 12292
  70.8 4.5 %copy-start.31 = (f32[4,128]{1,0:T(4,128)S(1)}, f32[4,128]{1,0:T(4,128)}, u32[]{:S(2)}) copy-start(f32[4,128]{1,0:T(4,128)} %param.33) | copy-start | bytes 6148
  70.8 4.5 %copy-start.16 = (bf16[3,128]{0,1:T(8,128)(2,1)S(1)}, bf16[3,128]{0,1:T(8,128)(2,1)}, u32[]{:S(2)}) copy-start(bf16[3,128]{0,1:T(8,128)(2,1)} %get-tuple-element.16) | copy-start | bytes 2308
  70.8 4.6 %copy-start.19 = (bf16[256,128]{1,0:T(8,128)(2,1)S(1)}, bf16[256,128]{1,0:T(8,128)(2,1)}, u32[]{:S(2)}) copy-start(bf16[256,128]{1,0:T(8,128)(2,1)} %param.25) | copy-start | bytes 196612
  71.6 3.9 %copy-start.7 = (bf16[256,128]{1,0:T(8,128)(2,1)S(1)}, bf16[256,128]{1,0:T(8,128)(2,1)}, u32[]{:S(2)}) copy-start(bf16[256,128]{1,0:T(8,128)(2,1)} %copy-done.6) | copy-start | bytes 196612
  71.6 195.3 %all-gather.9.cloned.1.call-start = ((), (), s32[]{:S(2)}) async-start(), calls=%async_computation.4 | async-start | bytes 6127616 | tf_op jit(solution)/shard_map/all_gather | solution.py:40
  73.5 35.6 %copy-start.10 = (f32[1,4,64,128]{3,2,1,0:T(8,128)S(1)}, f32[1,4,64,128]{3,2,1,0:T(8,128)}, u32[]{:S(2)}) copy-start(f32[1,4,64,128]{3,2,1,0:T(8,128)} %get-tuple-element.7) | copy-start | bytes 393220
  75.0 34.5 %copy-start.17 = (bf16[2,128,4,64]{1,0,3,2:T(2,128)(2,1)S(1)}, bf16[2,128,4,64]{1,0,3,2:T(2,128)(2,1)}, u32[]{:S(2)}) copy-start(bf16[2,128,4,64]{1,0,3,2:T(2,128)(2,1)} %get-tuple-element.5) | copy-start | bytes 393220
  105.8 4.5 %copy-start.32 = (f32[256]{0:T(256)S(1)}, f32[256]{0:T(256)}, u32[]{:S(2)}) copy-start(f32[256]{0:T(256)} %param.34) | copy-start | bytes 3076
  109.1 74.8 %copy-start.8 = (bf16[2,2048,64]{1,2,0:T(8,128)(2,1)S(1)}, bf16[2,2048,64]{1,2,0:T(8,128)(2,1)}, u32[]{:S(2)}) copy-start(bf16[2,2048,64]{1,2,0:T(8,128)(2,1)} %param.40) | copy-start | bytes 1572868
  110.6 78.3 %copy-start.34 = (bf16[2,2048,64]{1,2,0:T(8,128)(2,1)S(1)}, bf16[2,2048,64]{1,2,0:T(8,128)(2,1)}, u32[]{:S(2)}) copy-start(bf16[2,2048,64]{1,2,0:T(8,128)(2,1)} %param.41) | copy-start | bytes 1572868
  183.9 5.0 %copy-start.1 = (bf16[2,768,2048]{2,1,0:T(8,128)(2,1)S(1)}, bf16[2,768,2048]{2,1,0:T(8,128)(2,1)}, u32[]{:S(2)}) copy-start(bf16[2,768,2048]{2,1,0:T(8,128)(2,1)} %all-gather.7.cloned.1.call-done) | copy-start | bytes 18874372
  285.3 6.9 %copy-start.11 = (bf16[2,1024,128]{2,1,0:T(8,128)(2,1)S(1)}, bf16[2,1024,128]{2,1,0:T(8,128)(2,1)}, u32[]{:S(2)}) copy-start(bf16[2,1024,128]{2,1,0:T(8,128)(2,1)} %param.42) | copy-start | bytes 1572868
  292.2 17.7 %copy-start.28 = (f32[256,4]{0,1:T(4,128)S(1)}, f32[256,4]{0,1:T(4,128)}, u32[]{:S(2)}) copy-start(f32[256,4]{0,1:T(4,128)} %param.39) | copy-start | bytes 12292
  292.2 17.7 %copy-start.22 = (s32[1,256]{1,0:T(1,128)S(1)}, s32[1,256]{1,0:T(1,128)}, u32[]{:S(2)}) copy-start(s32[1,256]{1,0:T(1,128)} %copy-done.21) | copy-start | bytes 3076
  292.2 17.7 %copy-start.24 = (s32[1,256]{1,0:T(1,128)S(1)}, s32[1,256]{1,0:T(1,128)}, u32[]{:S(2)}) copy-start(s32[1,256]{1,0:T(1,128)} %copy-done.23) | copy-start | bytes 3076
  292.2 17.7 %copy-start.26 = (s32[1,256]{1,0:T(1,128)S(1)}, s32[1,256]{1,0:T(1,128)}, u32[]{:S(2)}) copy-start(s32[1,256]{1,0:T(1,128)} %copy-done.25) | copy-start | bytes 3076
  292.2 17.7 %copy-start.13 = (f32[64,256]{1,0:T(8,128)S(1)}, f32[64,256]{1,0:T(8,128)}, u32[]{:S(2)}) copy-start(f32[64,256]{1,0:T(8,128)} %copy-done.12) | copy-start | bytes 196612
  292.2 17.7 %copy-start.30 = (f32[24]{0:T(128)S(1)}, f32[24]{0:T(128)}, u32[]{:S(2)}) copy-start(f32[24]{0:T(128)} %copy-done.29) | copy-start | bytes 292
  296.6 40.9 %all-to-all-start.1 = ((bf16[2,768,128]{2,0,1:T(2,128)(2,1)}), bf16[2,768,128]{2,0,1:T(2,128)(2,1)S(1)}, u32[]{:S(2)}, u32[]{:S(2)}) async-start(bf16[2,768,128]{2,0,1:T(2,128)(2,1)} %copy.185), calls=%async_computation.1 | async-start | bytes 786432 | tf_op jit(solution)/shard_map/all_to_all | solution.py:222
  311.7 3.1 slice-start
  321.6 16.1 %copy-start.3 = (bf16[64,24,256]{2,1,0:T(8,128)(2,1)S(1)}, bf16[64,24,256]{2,1,0:T(8,128)(2,1)}, u32[]{:S(2)}) copy-start(bf16[64,24,256]{2,1,0:T(8,128)(2,1)} %get-tuple-element.18) | copy-start | bytes 2359300
  324.6 13.4 %copy-start.4 = (bf16[64,24,256]{2,1,0:T(8,128)(2,1)S(1)}, bf16[64,24,256]{2,1,0:T(8,128)(2,1)}, u32[]{:S(2)}) copy-start(bf16[64,24,256]{2,1,0:T(8,128)(2,1)} %get-tuple-element.17) | copy-start | bytes 2359300
  324.6 13.9 %copy-start.5 = (bf16[256,16,64]{0,2,1:T(8,128)(2,1)S(1)}, bf16[256,16,64]{0,2,1:T(8,128)(2,1)}, u32[]{:S(2)}) copy-start(bf16[256,16,64]{0,2,1:T(8,128)(2,1)} %copy.188) | copy-start | bytes 1572868
  337.5 1.0 copy-start.14
Sparse Core Ops, SparseCore 0:
  24.3 80.0 all-gather.4
  107.4 76.4 all-gather.6
  192.2 74.6 all-gather.8

commit v2 on v1

--- a/solution.py
+++ b/solution.py
@@ -1,6 +1,9 @@
 import jax
 import jax.numpy as jnp
 from jax import lax
+from jax.experimental import pallas as pl
+from jax.experimental.layout import Layout, with_layout_constraint
+from jax.experimental.pallas import tpu as pltpu
 from jax.sharding import PartitionSpec as P
 
 HEAD_DIM = 64
@@ -27,22 +30,6 @@
     a = high(x)
     b = high(x - a)
     return a, b, x - a - b
-
-
-def laid_out(tiles, dim):
-    tiles = jnp.moveaxis(tiles, 0, dim)
-    dims = tiles.shape
-    return tiles.reshape(*dims[:dim], dims[dim] * dims[dim + 1], *dims[dim + 2 :])
-
-
-def one_gather(arrays, axis, dims):
-    ravelled = jnp.concatenate([a.reshape(-1) for a in arrays])
-    lines, at, finished = (lax.all_gather(ravelled, axis), 0, [])
-    for a, dim in zip(arrays, dims):
-        tiles = lines[:, at : at + a.size].reshape(-1, *a.shape)
-        finished.append(laid_out(tiles, dim))
-        at += a.size
-    return tuple(finished)
 
 
 def conv_silu(tail_rows, source, weights):
@@ -77,7 +64,24 @@
     return summed.reshape(heads, HEAD_DIM, STATE)
 
 
-def routes(index_t, weight_t, experts, capacity):
+SIDE = 4
+HALF = 12
+PADDED = 16
+ROW_GROUPS = [[SIDE * y + x for x in range(SIDE)] for y in range(SIDE)]
+COLUMN_GROUPS = [[SIDE * y + x for y in range(SIDE)] for x in range(SIDE)]
+
+
+def along(x, groups):
+    return lax.all_to_all(
+        x, "tp", split_axis=0, concat_axis=0, tiled=True, axis_index_groups=groups
+    )
+
+
+def shown_to_row(x):
+    return along(jnp.broadcast_to(x[None], (SIDE,) + x.shape), ROW_GROUPS)
+
+
+def places(index_t, weight_t, experts):
     rows = index_t.shape[1]
     ids = jnp.arange(experts, dtype=jnp.int32)[:, None]
     named = jnp.zeros((experts, rows), F32)
@@ -89,10 +93,137 @@
     at = jnp.arange(rows)
     earlier = (at[:, None] < at[None, :]).astype(BF16)
     place = jnp.dot(named.astype(BF16), earlier, preferred_element_type=F32)
-    place = jnp.where(named > 0.0, place, -1.0)
-    slots = jnp.arange(capacity, dtype=jnp.int32).astype(F32)[None, :, None]
-    taken = place[:, None, :] == slots
-    return taken, weight
+    return jnp.where(named > 0.0, place, -1.0), weight
+
+
+def slot_numbers(half):
+    i = jnp.arange(PADDED, dtype=jnp.int32)
+    return jnp.where(i < HALF, half * HALF + i, -7).astype(F32)
+
+
+def pre_kernel(x_ref, g_ref, u_ref, h_ref):
+    k = x_ref.shape[2]
+    dims = (((1,), (1,)), ((), ()))
+    gate = jnp.zeros(h_ref.shape, F32)
+    up = jnp.zeros(h_ref.shape, F32)
+    for n in range(SIDE):
+        x = x_ref[n]
+        g = g_ref[:, n * k : (n + 1) * k]
+        u = u_ref[:, n * k : (n + 1) * k]
+        gate = gate + lax.dot_general(x, g, dims, preferred_element_type=F32)
+        up = up + lax.dot_general(x, u, dims, preferred_element_type=F32)
+    h_ref[...] = (gate / (1.0 + jnp.exp(-gate)) * up).astype(BF16)
+
+
+def expert_hidden(x, g, u):
+    slots = x.shape[1]
+    ff, width = g.shape
+    step = 128
+    return pl.pallas_call(
+        pre_kernel,
+        grid=(slots // step,),
+        in_specs=[
+            pl.BlockSpec((SIDE, step, x.shape[2]), lambda i: (0, i, 0)),
+            pl.BlockSpec((ff, width), lambda i: (0, 0)),
+            pl.BlockSpec((ff, width), lambda i: (0, 0)),
+        ],
+        out_specs=pl.BlockSpec((step, ff), lambda i: (i, 0)),
+        out_shape=jax.ShapeDtypeStruct((slots, ff), BF16),
+        cost_estimate=pl.CostEstimate(
+            flops=4 * slots * ff * width, bytes_accessed=4 * 2**20, transcendentals=slots * ff
+        ),
+    )(x, g, u)
+
+
+def down_kernel(h_ref, w_ref, o_ref):
+    k = h_ref.shape[2]
+    for m in range(SIDE):
+        total = jnp.zeros(o_ref.shape[1:], F32)
+        for n in range(SIDE):
+            w = w_ref[m, n * k : (n + 1) * k, :]
+            total = total + jnp.dot(h_ref[n], w, preferred_element_type=F32)
+        o_ref[m] = total.astype(BF16)
+
+
+def expert_down(h, w):
+    slots = h.shape[1]
+    width, columns = w.shape[1:]
+    step = 128
+    return pl.pallas_call(
+        down_kernel,
+        grid=(slots // step,),
+        in_specs=[
+            pl.BlockSpec((SIDE, step, h.shape[2]), lambda i: (0, i, 0)),
+            pl.BlockSpec(w.shape, lambda i: (0, 0, 0)),
+        ],
+        out_specs=pl.BlockSpec((SIDE, step, columns), lambda i: (0, i, 0)),
+        out_shape=jax.ShapeDtypeStruct((SIDE, slots, columns), BF16),
+        cost_estimate=pl.CostEstimate(
+            flops=2 * SIDE * slots * width * columns, bytes_accessed=3 * 2**20, transcendentals=0
+        ),
+    )(h, w)
+
+
+def last_kernel(g_ref, w_ref, s_ref, m_ref, r_ref, m_acc, r_acc):
+    n, _, lanes = g_ref.shape
+    rows = m_ref.shape[0]
+
+    @pl.when(pl.program_id(0) == 0)
+    def _():
+        m_acc[...] = jnp.zeros_like(m_acc)
+        r_acc[...] = jnp.zeros_like(r_acc)
+
+    mix = m_acc[...]
+    shared = r_acc[...]
+    half = lanes // 2
+    for t in range(n):
+        for c in range(2):
+            at = (2 * t + c) * lanes
+            piece = g_ref[t, c * rows : (c + 1) * rows, :]
+            mix = mix + jnp.dot(piece, w_ref[at : at + lanes, :], preferred_element_type=F32)
+        pair = g_ref[t, 2 * rows :, :]
+        w = s_ref[t * half : (t + 1) * half, :]
+        parts = [
+            jnp.dot(pair[:, c * half : (c + 1) * half], w, preferred_element_type=F32)
+            for c in range(2)
+        ]
+        shared = shared + jnp.concatenate(parts, axis=0)
+    m_acc[...] = mix
+    r_acc[...] = shared
+
+    @pl.when(pl.program_id(0) == pl.num_programs(0) - 1)
+    def _():
+        m_ref[...] = mix.astype(BF16)
+        r_ref[...] = shared
+
+
+def last_products(gathered, mix_weight, shared_weight, rows):
+    count, tall, lanes = gathered.shape
+    columns = mix_weight.shape[1]
+    n = 4
+    return pl.pallas_call(
+        last_kernel,
+        grid=(count // n,),
+        in_specs=[
+            pl.BlockSpec((n, tall, lanes), lambda i: (i, 0, 0)),
+            pl.BlockSpec((n * 2 * lanes, columns), lambda i: (i, 0)),
+            pl.BlockSpec((n * lanes // 2, columns), lambda i: (i, 0)),
+        ],
+        out_specs=[
+            pl.BlockSpec((rows, columns), lambda i: (0, 0)),
+            pl.BlockSpec((rows, columns), lambda i: (0, 0)),
+        ],
+        out_shape=[
+            jax.ShapeDtypeStruct((rows, columns), BF16),
+            jax.ShapeDtypeStruct((rows, columns), F32),
+        ],
+        scratch_shapes=[pltpu.VMEM((rows, columns), F32), pltpu.VMEM((rows, columns), F32)],
+        cost_estimate=pl.CostEstimate(
+            flops=2 * rows * columns * (mix_weight.shape[0] + shared_weight.shape[0]),
+            bytes_accessed=4 * 2**20,
+            transcendentals=0,
+        ),
+    )(gathered, mix_weight, shared_weight)
 
 
 def on_device(
@@ -188,50 +319,81 @@
     local_experts = routed_gate_weight.shape[0]
     ep_count = lax.axis_size("ep")
     experts = local_experts * ep_count
-    capacity = max(2, 3 * rows_local * TOP_K // (2 * experts))
-    col_width = model_width // lax.axis_size("tp")
+    tp_place = lax.axis_index("tp")
+    down, across = tp_place // SIDE, tp_place % SIDE
+    my_expert, my_half = down // 2, down % 2
+    columns = routed_down_weight.shape[2]
+    part_ff = routed_gate_weight.shape[2]
+    share = model_width // SIDE
+
+    gate_up = jnp.stack(
+        [jnp.swapaxes(routed_gate_weight, 1, 2), jnp.swapaxes(routed_up_weight, 1, 2)]
+    )
+    gate_up = jnp.concatenate([gate_up[0], gate_up[1]], axis=1)
+    gate_up = jnp.stack([gate_up[0], gate_up[0], gate_up[1], gate_up[1]])
+    gate_up = along(gate_up, COLUMN_GROUPS)
+    gate_w = gate_up[:, :part_ff].reshape(SIDE * part_ff, model_width)
+    up_w = gate_up[:, part_ff:].reshape(SIDE * part_ff, model_width)
+    down_w = routed_down_weight.reshape(local_experts, SIDE, SIDE, part_ff, columns)
+    down_w = jnp.swapaxes(down_w, 1, 2).reshape(routed_down_weight.shape)
+    down_w = along(jnp.stack([down_w[0], down_w[0], down_w[1], down_w[1]]), COLUMN_GROUPS)
+
     rows_wide = second_token_rows.astype(F32)
     normed = (
         rows_wide
         * lax.rsqrt(jnp.mean(rows_wide * rows_wide, axis=-1, keepdims=True) + epsilon)
         * expert_norm_scale
     ).astype(BF16)
-    taken, weight = routes(routed_expert_index.T, routed_expert_weight.T, experts, capacity)
-    one_hot = taken.astype(BF16).reshape(experts * capacity, rows_local)
-    mine = lax.dynamic_slice_in_dim(normed, lax.axis_index("tp") * col_width, col_width, 1)
-    my_columns = jnp.dot(one_hot, mine, preferred_element_type=F32).astype(BF16)
-    my_columns = my_columns.reshape(experts, capacity, col_width)
-    arrived = lax.all_to_all(my_columns, "ep", split_axis=0, concat_axis=1, tiled=True)
-    column_piece = lax.all_gather(arrived, "tp", axis=2, tiled=True)
-    gate_pre = jnp.einsum(
-        "esd,edf->esf", column_piece, routed_gate_weight, preferred_element_type=F32
-    )
-    up_pre = jnp.einsum("esd,edf->esf", column_piece, routed_up_weight, preferred_element_type=F32)
-    hidden = (jax.nn.silu(gate_pre) * up_pre).astype(BF16)
+    place, weight = places(routed_expert_index.T, routed_expert_weight.T, experts)
+    by_owner = place.reshape(ep_count, local_experts, rows_local)
+    mine = lax.dynamic_index_in_dim(by_owner, my_expert, 1, False)
+    taken = mine[:, None, :] == slot_numbers(my_half)[None, :, None]
+    one_hot = taken.astype(BF16).reshape(ep_count * PADDED, rows_local)
+    my_share = lax.dynamic_slice_in_dim(normed, across * share, share, 1)
+    outgoing = jnp.dot(one_hot, my_share, preferred_element_type=F32).astype(BF16)
+    arrived = lax.all_to_all(
+        outgoing.reshape(ep_count, PADDED, share), "ep", split_axis=0, concat_axis=0, tiled=True
+    )
+    arrived = shown_to_row(arrived.reshape(ep_count * PADDED, share))
+    hidden = shown_to_row(expert_hidden(arrived, gate_w, up_w))
+    result = along(expert_down(hidden, down_w), COLUMN_GROUPS)
+    result = jnp.swapaxes(result.reshape(SIDE, ep_count, PADDED, columns), 0, 1)
+    result = result.reshape(ep_count, SIDE * PADDED, columns)
+    returned = lax.all_to_all(result, "ep", split_axis=0, concat_axis=0, tiled=True)
+    returned = returned.reshape(ep_count * SIDE * PADDED, columns)
+
     shared_hidden = (
         jax.nn.silu(jnp.dot(normed, shared_gate_weight, preferred_element_type=F32))
         * jnp.dot(normed, shared_up_weight, preferred_element_type=F32)
     ).astype(BF16)
-    whole_mix, whole_hidden, whole_shared = one_gather(
-        (mixer_normed, hidden, shared_hidden), "tp", (1, 2, 1)
-    )
-    mixer_output = jnp.dot(whole_mix, mixer_output_weight, preferred_element_type=F32).astype(BF16)
-    expert_result = jnp.einsum(
-        "esf,efd->esd", whole_hidden, routed_down_weight, preferred_element_type=F32
-    ).astype(BF16)
-    returned = lax.all_to_all(expert_result, "ep", split_axis=1, concat_axis=0, tiled=True)
-    returned = returned.reshape(experts * capacity, col_width)
+    half_rows = rows_local // 2
+    lanes = width_x // 2
+    payload = jnp.concatenate(
+        [
+            mixer_normed[:, :lanes],
+            mixer_normed[:, lanes:],
+            jnp.concatenate([shared_hidden[:half_rows], shared_hidden[half_rows:]], axis=1),
+        ],
+        axis=0,
+    )
+    payload = with_layout_constraint(payload, Layout(major_to_minor=(0, 1)))
+    gathered = lax.all_gather(payload, "tp")
+    mixer_output, shared_result = last_products(
+        gathered, mixer_output_weight, shared_down_weight, rows_local
+    )
+
+    halves = jnp.stack([slot_numbers(0), slot_numbers(1)])
+    taken = by_owner[:, :, None, None, :] == halves[None, None, :, :, None]
+    weight = weight.reshape(ep_count, local_experts, 1, 1, rows_local)
     weight_high = high(weight)
     contract = (((0,), (0,)), ((), ()))
-    routed_sum = jnp.zeros((rows_local, col_width), F32)
+    routed_sum = shared_result
     for part in (weight_high, weight - weight_high):
-        spread_part = jnp.where(taken, part[:, None, :], 0.0).astype(BF16)
-        spread_part = spread_part.reshape(experts * capacity, rows_local)
+        spread_part = jnp.where(taken, part, 0.0).astype(BF16).reshape(-1, rows_local)
         routed_sum = routed_sum + lax.dot_general(
             spread_part, returned, contract, preferred_element_type=F32
         )
-    shared_result = jnp.dot(whole_shared, shared_down_weight, preferred_element_type=F32)
-    routed_out = (routed_sum + shared_result).astype(BF16)
+    routed_out = routed_sum.astype(BF16)
     return (mixer_output, routed_out)
 
 

time: 347 us -> 271 us (0.78)
  waiting for transfers between devices: 190 us -> 95.2 us
  starting transfers between devices: 18.2 us -> 48.2 us
  local copies, waits for them, and re-layouts: 46.7 us -> 24.8 us
  Pallas kernels: 0 us -> 14.7 us
  other arithmetic: 12.5 us -> 23.9 us
  matrix products: 19.5 us -> 10.3 us
  blocking collectives: 44.8 us -> 37.5 us
    all_gather x2 -> x1, waiting for transfers between devices: 148 us -> 0.02 us  [on_device(): gathered = lax.all_gather(payload, 'tp')]
    all_to_all x1 -> x5, waiting for transfers between devices: 12.9 us -> 66.4 us  [the longest x3 38.4 us: along(): lax.all_to_all(x, 'tp', split_axis=0, concat_axis=0, tiled=True, axis_ind...]
    all_to_all x1 -> x5, starting transfers between devices: 13.2 us -> 43.2 us  [the longest x1 17.9 us: on_device(): lax.all_to_all(outgoing.reshape(ep_count, PADDED, share), 'ep', split_axi...]
    pallas_call x0 -> x3, Pallas kernels: none -> 14.7 us  [the longest x1 5.98 us: expert_hidden(): pl.pallas_call(pre_kernel, grid=(slots // step,), in_specs=[pl.BlockSpec(...]
    dot_general x7 -> x2, matrix products: 14.8 us -> 2.86 us  [the longest x1 2.06 us: on_device(): jnp.dot(one_hot, my_share, preferred_element_type=F32).astype(BF16)]
    transpose x3 -> x0, local copies, waits for them, and re-layouts: 10.4 us -> none  [laid_out(): tiles = jnp.moveaxis(tiles, 0, dim)]
    all_to_all x1 -> x2, blocking collectives: 44.8 us -> 37.5 us  [along(): lax.all_to_all(x, 'tp', split_axis=0, concat_axis=0, tiled=True, axis_ind...]
    reshape x4, local copies, waits for them, and re-layouts: 10.3 us -> 3.3 us  [the longest x2 2.4 us: on_device(): mixed_heads = (inside + carried_term).reshape(length, heads_local, HEAD_DIM)]
  transfers between devices with their start and end apart: 5 -> 8, of which waited for: 4 -> 5; matrix products, arithmetic and copies ran while one was open for 9% -> 18% of each run, Pallas kernels for 0% -> 5%
where the time goes in v2:
time: 271 us; the launch traced here: 269 us
  waiting for transfers between devices  95.2 us (35%)
  starting transfers between devices  48.2 us (18%)
  blocking collectives  37.5 us (14%)
  local copies, waits for them, and re-layouts  24.8 us (9%)
  other arithmetic  23.9 us (9%)
  Pallas kernels  14.7 us (5%)
  between operations  14.6 us (5%)
  matrix products  10.3 us (4%)
    all_to_all x3, waiting for transfers between devices, along(): lax.all_to_all(x, 'tp', split_axis=0, concat_axis=0, tiled=True, axis_ind...  38.4 us
    all_to_all x2, blocking collectives, along(): lax.all_to_all(x, 'tp', split_axis=0, concat_axis=0, tiled=True, axis_ind...  37.5 us
    all_gather x1, waiting for transfers between devices, state_before(): gathered = lax.all_gather(payload, 'ep')  28.7 us
    all_to_all x1, waiting for transfers between devices, on_device(): lax.all_to_all(result, 'ep', split_axis=0, concat_axis=0, tiled=True)  28.1 us
    all_to_all x1, starting transfers between devices, on_device(): lax.all_to_all(outgoing.reshape(ep_count, PADDED, share), 'ep', split_axi...  17.9 us
    all_to_all x1, starting transfers between devices, on_device(): lax.all_to_all(result, 'ep', split_axis=0, concat_axis=0, tiled=True)  12.8 us
    all_to_all x3, starting transfers between devices, along(): lax.all_to_all(x, 'tp', split_axis=0, concat_axis=0, tiled=True, axis_ind...  12.4 us
    pallas_call x1, Pallas kernels, expert_hidden(): pl.pallas_call(pre_kernel, grid=(slots // step,), in_specs=[pl.BlockSpec(...  5.98 us
  transfers between devices with their start and end apart: 8, of which 5 were waited for; matrix products, arithmetic and copies ran while one was open for 18% of the time, Pallas kernels for 5%

profile of v2, /device:TPU:1, one launch (start us, length us, event | category | flops | bytes accessed | tf_op | source)
XLA Modules:
  0.0 269.2 jit_solution(2446490820970965116)
XLA Ops:
  9.3 4.9 %collective-permute-start = (bf16[3,512]{1,0:T(4,128)(2,1)S(1)}, bf16[3,512]{1,0:T(4,128)(2,1)S(1)}, u32[]{:S(2)}, u32[]{:S(2)}) collective-permute-start(bf16[3,512]{1,0:T(4,128)(2,1)S(1)} %pad_maximum_fusion.5), channel_id=1, source_target_pairs={{0,16},{16,32},{32,48},{48,64},{64,80},{80,96},{96,112},{112,128},... | collective-permute-start | bytes 9224 | tf_op jit(solution)/shard_map/ppermute | solution.py:22
  16.1 0.8 fusion.81
  17.6 0.8 slice_bitcast_fusion.3
  19.0 1.4 fusion.43
  20.7 0.8 broadcast_multiply_fusion
  24.1 1.5 fusion.8
  25.6 4.3 %all-to-all-start.2 = ((bf16[4,128,2048]{2,1,0:T(8,128)(2,1)}), bf16[4,128,2048]{2,1,0:T(8,128)(2,1)S(1)}, u32[]{:S(2)}, u32[]{:S(2)}) async-start(bf16[4,128,2048]{2,1,0:T(8,128)(2,1)} %fusion.8), calls=%async_computation.2 | async-start | bytes 4194304 | tf_op jit(solution)/shard_map/all_to_all | solution.py:75
  30.5 0.8 convolution_select_fusion
  31.3 1.5 eq.214
  33.1 1.5 fusion.4
  35.9 1.4 copy.136
  38.0 1.6 bitcast_compare_fusion
  39.6 2.1 convolution_convert_fusion
  41.6 1.2 subtract_exponential_fusion.1
  42.9 1.4 slice_bitcast_fusion.7
  45.3 1.1 fusion.11
  46.4 7.4 %all-to-all-done.2 = bf16[4,128,2048]{2,1,0:T(8,128)(2,1)S(1)} async-done(((bf16[4,128,2048]{2,1,0:T(8,128)(2,1)}), bf16[4,128,2048]{2,1,0:T(8,128)(2,1)S(1)}, u32[]{:S(2)}, u32[]{:S(2)}) %all-to-all-start.2) | async-done | bytes 2097184 | tf_op jit(solution)/shard_map/all_to_all | solution.py:75
  53.8 17.9 %all-to-all-start = ((bf16[32,16,512]{2,1,0:T(8,128)(2,1)}), bf16[32,16,512]{2,1,0:T(8,128)(2,1)S(1)}, u32[]{:S(2)}, u32[]{:S(2)}) async-start(bf16[32,16,512]{2,1,0:T(8,128)(2,1)} %bitcast.121), calls=%async_computation | async-start | bytes 1048576 | tf_op jit(solution)/shard_map/all_to_all | solution.py:354
  71.7 1.0 copy.112
  74.7 1.4 fusion.77
  76.1 1.1 multiply_convert_fusion.3
  77.2 1.7 fusion.82
  78.9 28.7 %all-gather.4.cloned.1.call-done = bf16[32,272,128]{2,1,0:T(8,128)(2,1)} async-done(((bf16[1,272,128]{2,1,0:T(8,128)(2,1)}), bf16[32,272,128]{2,1,0:T(8,128)(2,1)}) %all-gather.4.cloned.1.call-update) | async-done | bytes 2228240 | tf_op jit(solution)/shard_map/all_gather | solution.py:55
  107.6 0.8 slice.246
  110.3 3.2 %multiply_reduce_fusion = f32[256,128]{1,0:T(8,128)S(1)} fusion(bf16[32,272,128]{2,1,0:T(8,128)(2,1)} %all-gather.4.cloned.1.call-done, f32[32,256]{1,0:T(8,128)S(1)} %mul.344), kind=kLoop, calls=%fused_computation.3 | loop fusion | flops 3112960 | bytes 2260992 | tf_op jit(solution)/shard_map/reduce_sum | solution.py:63
  113.9 1.3 fusion.10
  115.1 1.0 copy.125
  116.2 1.4 reshape.577
  117.6 1.4 multiply_reduce_fusion.1
  119.0 1.5 broadcast_in_dim.192
  120.5 4.6 %all-to-all-start.1 = ((bf16[4,512,512]{2,1,0:T(8,128)(2,1)}), bf16[4,512,512]{2,1,0:T(8,128)(2,1)}, u32[]{:S(2)}, u32[]{:S(2)}) async-start(bf16[4,512,512]{2,1,0:T(8,128)(2,1)} %broadcast_in_dim.192), calls=%async_computation.1 | async-start | bytes 4194304 | tf_op jit(solution)/shard_map/all_to_all | solution.py:75
  126.2 1.2 pad_maximum_fusion
  127.4 25.0 %all-to-all-done.1.x_ref = bf16[4,512,512]{2,1,0:T(8,128)(2,1)} async-done(((bf16[4,512,512]{2,1,0:T(8,128)(2,1)}), bf16[4,512,512]{2,1,0:T(8,128)(2,1)}, u32[]{:S(2)}, u32[]{:S(2)}) %all-to-all-start.1) | async-done | bytes 2097184 | tf_op jit(solution)/shard_map/all_to_all | solution.py:75
  152.4 3.5 %all-to-all-start.4 = ((bf16[4,1024,128]{2,1,0:T(8,128)(2,1)}), bf16[4,1024,128]{2,1,0:T(8,128)(2,1)S(1)}, u32[]{:S(2)}, u32[]{:S(2)}) async-start(bf16[4,1024,128]{2,1,0:T(8,128)(2,1)} %pad_maximum_fusion), calls=%async_computation.4 | async-start | bytes 2097152 | tf_op jit(solution)/shard_map/all_to_all | solution.py:75
  156.0 1.5 fusion.72
  157.5 6.0 %shard_map.231 = bf16[512,256]{1,0:T(8,128)(2,1)} custom-call(bf16[4,512,512]{2,1,0:T(8,128)(2,1)} %all-to-all-done.1.x_ref, bf16[256,2048]{1,0:T(8,128)(2,1)} %bitcast.114, bf16[256,2048]{1,0:T(8,128)(2,1)} %bitcast.113), custom_call_target="tpu_custom_call" | custom-call | flops 1073741824 | bytes 4194304 | tf_op jit(solution)/shard_map/pallas_call | solution.py:122
  163.4 6.0 %all-to-all-done.4.w_ref = bf16[4,1024,128]{2,1,0:T(8,128)(2,1)S(1)} async-done(((bf16[4,1024,128]{2,1,0:T(8,128)(2,1)}), bf16[4,1024,128]{2,1,0:T(8,128)(2,1)S(1)}, u32[]{:S(2)}, u32[]{:S(2)}) %all-to-all-start.4) | async-done | bytes 1048608 | tf_op jit(solution)/shard_map/all_to_all | solution.py:75
  169.4 1.2 broadcast_in_dim.193
  170.6 26.4 %all_to_all.35.h_ref = bf16[4,512,256]{2,1,0:T(8,128)(2,1)} all-to-all(bf16[4,512,256]{2,1,0:T(8,128)(2,1)S(1)} %broadcast_in_dim.193), channel_id=1, replica_groups={{0,1,2,3},{4,5,6,7},{8,9,10,11},{12,13,14,15},{16,17,18,19},{20,21,22,2..., dimensions={0} | all-to-all | bytes 2097152 | tf_op jit(solution)/shard_map/all_to_all | solution.py:75
  197.0 4.5 %shard_map.232 = bf16[4,512,128]{2,1,0:T(8,128)(2,1)} custom-call(bf16[4,512,256]{2,1,0:T(8,128)(2,1)} %all_to_all.35.h_ref, bf16[4,1024,128]{2,1,0:T(8,128)(2,1)} %copy-done.2), custom_call_target="tpu_custom_call" | custom-call | flops 536870912 | bytes 3145728 | tf_op jit(solution)/shard_map/pallas_call | solution.py:152
  201.5 11.1 %all_to_all.36 = bf16[4,512,128]{2,1,0:T(8,128)(2,1)S(1)} all-to-all(bf16[4,512,128]{2,1,0:T(8,128)(2,1)} %shard_map.232), channel_id=1, replica_groups={{0,4,8,12},{1,5,9,13},{2,6,10,14},{3,7,11,15},{16,20,24,28},{17,21,25,2..., dimensions={0} | all-to-all | bytes 1048576 | tf_op jit(solution)/shard_map/all_to_all | solution.py:75
  212.6 0.9 copy.121
  213.5 12.8 %all-to-all-start.6 = ((bf16[32,64,128]{2,1,0:T(8,128)(2,1)}), bf16[32,64,128]{2,1,0:T(8,128)(2,1)S(1)}, u32[]{:S(2)}, u32[]{:S(2)}) async-start(bf16[32,64,128]{2,1,0:T(8,128)(2,1)} %bitcast.53), calls=%async_computation.6 | async-start | bytes 1048576 | tf_op jit(solution)/shard_map/all_to_all | solution.py:362
  226.6 0.9 fusion.6
  227.5 4.3 %shard_map.230 = (bf16[256,128]{1,0:T(8,128)(2,1)}, f32[256,128]{1,0:T(8,128)}) custom-call(bf16[16,640,128]{2,1,0:T(8,128)(2,1)} %bitcast.115, bf16[4096,128]{1,0:T(8,128)(2,1)} %w_ref.1, bf16[1024,128]{1,0:T(8,128)(2,1)} %s_ref.1), custom_call_target="tpu_custom_call" | custom-call | flops 335544320 | bytes 4194304 | tf_op jit(solution)/shard_map/pallas_call | solution.py:204
  231.7 28.1 %all-to-all-done.6 = bf16[32,64,128]{2,1,0:T(8,128)(2,1)S(1)} async-done(((bf16[32,64,128]{2,1,0:T(8,128)(2,1)}), bf16[32,64,128]{2,1,0:T(8,128)(2,1)S(1)}, u32[]{:S(2)}, u32[]{:S(2)}) %all-to-all-start.6) | async-done | bytes 524320 | tf_op jit(solution)/shard_map/all_to_all | solution.py:362
  259.8 1.4 convolution_add_fusion.1
  261.2 1.1 fusion.12
  (143 shorter events, 17.2 us)
Async XLA Ops:
  7.2 37.7 %copy-start = (bf16[2048,64]{0,1:T(8,128)(2,1)S(1)}, bf16[2048,64]{0,1:T(8,128)(2,1)}, u32[]{:S(2)}) copy-start(bf16[2048,64]{0,1:T(8,128)(2,1)} %param.43) | copy-start | bytes 786436
  7.2 15.0 %copy-start.17 = (bf16[256,128]{1,0:T(8,128)(2,1)S(1)}, bf16[256,128]{1,0:T(8,128)(2,1)}, u32[]{:S(2)}) copy-start(bf16[256,128]{1,0:T(8,128)(2,1)} %param.24) | copy-start | bytes 196612
  7.2 100.4 %all-gather.4.cloned.1.call-start = ((), (), s32[]{:S(2)}) async-start(), calls=%async_computation.7 | async-start | bytes 2297856 | tf_op jit(solution)/shard_map/all_gather | solution.py:55
  9.3 9.6 %collective-permute-start = (bf16[3,512]{1,0:T(4,128)(2,1)S(1)}, bf16[3,512]{1,0:T(4,128)(2,1)S(1)}, u32[]{:S(2)}, u32[]{:S(2)}) collective-permute-start(bf16[3,512]{1,0:T(4,128)(2,1)S(1)} %pad_maximum_fusion.5), channel_id=1, source_target_pairs={{0,16},{16,32},{32,48},{48,64},{64,80},{80,96},{96,112},{112,128},... | collective-permute-start | bytes 9224 | tf_op jit(solution)/shard_map/ppermute | solution.py:22
  16.1 19.3 %copy-start.18 = (f32[2,1,4]{2,1,0:T(1,128)}, f32[2,1,4]{2,1,0:T(1,128)S(1)}, u32[]{:S(2)}) copy-start(f32[2,1,4]{2,1,0:T(1,128)S(1)} %get-tuple-element.22) | copy-start | bytes 100
  17.6 6.4 %copy-start.5 = (bf16[2,2048,64]{1,2,0:T(8,128)(2,1)S(1)}, bf16[2,2048,64]{1,2,0:T(8,128)(2,1)}, u32[]{:S(2)}) copy-start(bf16[2,2048,64]{1,2,0:T(8,128)(2,1)} %param.41) | copy-start | bytes 1572868
  17.6 6.4 %copy-start.6 = (bf16[2,2048,64]{1,2,0:T(8,128)(2,1)S(1)}, bf16[2,2048,64]{1,2,0:T(8,128)(2,1)}, u32[]{:S(2)}) copy-start(bf16[2,2048,64]{1,2,0:T(8,128)(2,1)} %param.40) | copy-start | bytes 1572868
  20.4 3.7 %copy-start.3 = (f32[256,256]{1,0:T(8,128)}, f32[256,256]{1,0:T(8,128)S(1)}, u32[]{:S(2)}) copy-start(f32[256,256]{1,0:T(8,128)S(1)} %fusion.43) | copy-start | bytes 786436
  22.2 3.3 %copy-start.8 = (bf16[256,128]{1,0:T(8,128)(2,1)}, bf16[256,128]{1,0:T(8,128)(2,1)S(1)}, u32[]{:S(2)}) copy-start(bf16[256,128]{1,0:T(8,128)(2,1)S(1)} %multiply_convert_fusion.2) | copy-start | bytes 196612
  25.6 4.3 %copy-start.30 = (s32[256,4]{0,1:T(4,128)S(1)}, s32[256,4]{0,1:T(4,128)}, u32[]{:S(2)}) copy-start(s32[256,4]{0,1:T(4,128)} %param.38) | copy-start | bytes 12292
  25.6 7.2 %copy-start.1 = (bf16[256,2048]{1,0:T(8,128)(2,1)S(1)}, bf16[256,2048]{1,0:T(8,128)(2,1)}, u32[]{:S(2)}) copy-start(bf16[256,2048]{1,0:T(8,128)(2,1)} %param.36) | copy-start | bytes 3145732
  25.6 7.5 %copy-start.19 = (f32[2048]{0:T(1024)S(1)}, f32[2048]{0:T(1024)}, u32[]{:S(2)}) copy-start(f32[2048]{0:T(1024)} %param.37) | copy-start | bytes 24580
  25.6 28.2 %all-to-all-start.2 = ((bf16[4,128,2048]{2,1,0:T(8,128)(2,1)}), bf16[4,128,2048]{2,1,0:T(8,128)(2,1)S(1)}, u32[]{:S(2)}, u32[]{:S(2)}) async-start(bf16[4,128,2048]{2,1,0:T(8,128)(2,1)} %fusion.8), calls=%async_computation.2 | async-start | bytes 4194304 | tf_op jit(solution)/shard_map/all_to_all | solution.py:75
  29.9 0.5 copy-start.21
  29.9 0.5 copy-start.23
  29.9 0.6 copy-start.25
  30.0 0.6 copy-start.27
  32.8 1.8 copy-start.11
  39.6 5.8 %copy-start.34 = (bf16[2048,64]{0,1:T(8,128)(2,1)S(1)}, bf16[2048,64]{0,1:T(8,128)(2,1)}, u32[]{:S(2)}) copy-start(bf16[2048,64]{0,1:T(8,128)(2,1)} %param.44) | copy-start | bytes 786436
  39.6 4.7 %copy-start.32 = (pred[32]{0:T(512)(128)(4,1)}, pred[32]{0:T(512)(128)(4,1)S(1)}, u32[]{:S(2)}) copy-start(pred[32]{0:T(512)(128)(4,1)S(1)} %iota_compare_fusion.9) | copy-start | bytes 100
  53.7 59.8 %copy-start.10 = (f32[1,4,64,128]{3,2,1,0:T(8,128)S(1)}, f32[1,4,64,128]{3,2,1,0:T(8,128)}, u32[]{:S(2)}) copy-start(f32[1,4,64,128]{3,2,1,0:T(8,128)} %get-tuple-element.15) | copy-start | bytes 393220
  53.7 59.8 %copy-start.20 = (f32[2,4]{1,0:T(2,128)S(1)}, f32[2,4]{1,0:T(2,128)}, u32[]{:S(2)}) copy-start(f32[2,4]{1,0:T(2,128)} %subtract_exponential_fusion.1) | copy-start | bytes 100
  53.8 65.2 %all-to-all-start = ((bf16[32,16,512]{2,1,0:T(8,128)(2,1)}), bf16[32,16,512]{2,1,0:T(8,128)(2,1)S(1)}, u32[]{:S(2)}, u32[]{:S(2)}) async-start(bf16[32,16,512]{2,1,0:T(8,128)(2,1)} %bitcast.121), calls=%async_computation | async-start | bytes 1048576 | tf_op jit(solution)/shard_map/all_to_all | solution.py:354
  110.3 3.6 %copy-start.14 = (f32[2,128,128]{2,1,0:T(8,128)S(1)}, f32[2,128,128]{2,1,0:T(8,128)}, u32[]{:S(2)}) copy-start(f32[2,128,128]{2,1,0:T(8,128)} %fusion.82) | copy-start | bytes 393220
  110.3 3.6 %copy-start.29 = (f32[2,4,128]{2,1,0:T(4,128)S(1)}, f32[2,4,128]{2,1,0:T(4,128)}, u32[]{:S(2)}) copy-start(f32[2,4,128]{2,1,0:T(4,128)} %copy.105) | copy-start | bytes 12292
  113.5 4.1 %copy-start.4 = (f32[256,256]{1,0:T(8,128)S(1)}, f32[256,256]{1,0:T(8,128)}, u32[]{:S(2)}) copy-start(f32[256,256]{1,0:T(8,128)} %copy-done.3) | copy-start | bytes 786436
  113.5 4.0 %copy-start.13 = (bf16[256,256]{1,0:T(8,128)(2,1)S(1)}, bf16[256,256]{1,0:T(8,128)(2,1)}, u32[]{:S(2)}) copy-start(bf16[256,256]{1,0:T(8,128)(2,1)} %param.26) | copy-start | bytes 393220
  120.5 4.7 %copy-start.7 = (f32[256,256]{1,0:T(8,128)S(1)}, f32[256,256]{1,0:T(8,128)}, u32[]{:S(2)}) copy-start(f32[256,256]{1,0:T(8,128)} %get-tuple-element.7) | copy-start | bytes 786436
  120.5 4.7 %copy-start.33 = (f32[256]{0:T(256)S(1)}, f32[256]{0:T(256)}, u32[]{:S(2)}) copy-start(f32[256]{0:T(256)} %param.34) | copy-start | bytes 3076
  120.5 4.8 %copy-start.15 = (bf16[128,64]{1,0:T(8,128)(2,1)S(1)}, bf16[128,64]{1,0:T(8,128)(2,1)}, u32[]{:S(2)}) copy-start(bf16[128,64]{1,0:T(8,128)(2,1)} %get-tuple-element.27) | copy-start | bytes 49156
  120.5 4.8 %copy-start.16 = (bf16[128,64]{1,0:T(8,128)(2,1)S(1)}, bf16[128,64]{1,0:T(8,128)(2,1)}, u32[]{:S(2)}) copy-start(bf16[128,64]{1,0:T(8,128)(2,1)} %get-tuple-element.28) | copy-start | bytes 49156
  120.5 5.6 %copy-start.9 = (bf16[2,1024,128]{2,1,0:T(8,128)(2,1)S(1)}, bf16[2,1024,128]{2,1,0:T(8,128)(2,1)}, u32[]{:S(2)}) copy-start(bf16[2,1024,128]{2,1,0:T(8,128)(2,1)} %param.42) | copy-start | bytes 1572868
  120.5 31.9 %all-to-all-start.1 = ((bf16[4,512,512]{2,1,0:T(8,128)(2,1)}), bf16[4,512,512]{2,1,0:T(8,128)(2,1)}, u32[]{:S(2)}, u32[]{:S(2)}) async-start(bf16[4,512,512]{2,1,0:T(8,128)(2,1)} %broadcast_in_dim.192), calls=%async_computation.1 | async-start | bytes 4194304 | tf_op jit(solution)/shard_map/all_to_all | solution.py:75
  125.1 102.3 %all-gather.6.cloned.1.call-start = ((), (), s32[]{:S(2)}) async-start(), calls=%async_computation.8 | async-start | bytes 2785280 | tf_op jit(solution)/shard_map/all_gather | solution.py:380
  152.4 17.0 %all-to-all-start.4 = ((bf16[4,1024,128]{2,1,0:T(8,128)(2,1)}), bf16[4,1024,128]{2,1,0:T(8,128)(2,1)S(1)}, u32[]{:S(2)}, u32[]{:S(2)}) async-start(bf16[4,1024,128]{2,1,0:T(8,128)(2,1)} %pad_maximum_fusion), calls=%async_computation.4 | async-start | bytes 2097152 | tf_op jit(solution)/shard_map/all_to_all | solution.py:75
  169.4 27.6 %copy-start.2 = (bf16[4,1024,128]{2,1,0:T(8,128)(2,1)}, bf16[4,1024,128]{2,1,0:T(8,128)(2,1)S(1)}, u32[]{:S(2)}) copy-start(bf16[4,1024,128]{2,1,0:T(8,128)(2,1)S(1)} %all-to-all-done.4.w_ref) | copy-start | bytes 3145732
  201.5 24.9 %copy-start.31 = (f32[256,4]{0,1:T(4,128)S(1)}, f32[256,4]{0,1:T(4,128)}, u32[]{:S(2)}) copy-start(f32[256,4]{0,1:T(4,128)} %param.39) | copy-start | bytes 12292
  201.5 24.9 %copy-start.22 = (s32[1,256]{1,0:T(1,128)S(1)}, s32[1,256]{1,0:T(1,128)}, u32[]{:S(2)}) copy-start(s32[1,256]{1,0:T(1,128)} %copy-done.21) | copy-start | bytes 3076
  201.5 24.9 %copy-start.24 = (s32[1,256]{1,0:T(1,128)S(1)}, s32[1,256]{1,0:T(1,128)}, u32[]{:S(2)}) copy-start(s32[1,256]{1,0:T(1,128)} %copy-done.23) | copy-start | bytes 3076
  201.5 24.9 %copy-start.26 = (s32[1,256]{1,0:T(1,128)S(1)}, s32[1,256]{1,0:T(1,128)}, u32[]{:S(2)}) copy-start(s32[1,256]{1,0:T(1,128)} %copy-done.25) | copy-start | bytes 3076
  201.5 24.9 %copy-start.28 = (s32[1,256]{1,0:T(1,128)S(1)}, s32[1,256]{1,0:T(1,128)}, u32[]{:S(2)}) copy-start(s32[1,256]{1,0:T(1,128)} %copy-done.27) | copy-start | bytes 3076
  201.5 25.1 %copy-start.12 = (f32[32,2,256]{2,1,0:T(2,128)S(1)}, f32[32,2,256]{2,1,0:T(2,128)}, u32[]{:S(2)}) copy-start(f32[32,2,256]{2,1,0:T(2,128)} %eq.214) | copy-start | bytes 196612
  213.5 46.4 %all-to-all-start.6 = ((bf16[32,64,128]{2,1,0:T(8,128)(2,1)}), bf16[32,64,128]{2,1,0:T(8,128)(2,1)S(1)}, u32[]{:S(2)}, u32[]{:S(2)}) async-start(bf16[32,64,128]{2,1,0:T(8,128)(2,1)} %bitcast.53), calls=%async_computation.6 | async-start | bytes 1048576 | tf_op jit(solution)/shard_map/all_to_all | solution.py:362
Sparse Core Ops, SparseCore 0:
  24.2 83.4 all-gather.3
  129.0 68.2 all-gather.5

commit v3 on v2

--- a/solution.py
+++ b/solution.py
@@ -2,7 +2,6 @@
 import jax.numpy as jnp
 from jax import lax
 from jax.experimental import pallas as pl
-from jax.experimental.layout import Layout, with_layout_constraint
 from jax.experimental.pallas import tpu as pltpu
 from jax.sharding import PartitionSpec as P
 
@@ -14,6 +13,13 @@
 epsilon = 1e-05
 F32 = jnp.float32
 BF16 = jnp.bfloat16
+
+
+def whole(shape):
+    return pl.BlockSpec(shape, lambda *_: (0,) * len(shape))
+
+
+SCALAR = pl.BlockSpec(memory_space=pltpu.SMEM)
 
 
 def passed_along(x, axis, by):
@@ -44,24 +50,99 @@
     return jax.nn.silu(total_sum).astype(BF16)
 
 
-def state_before(log_total, total_state):
+def states_gathered(log_total, total_state):
     heads = log_total.shape[0]
-    count = lax.axis_size("ep")
-    place = lax.axis_index("ep")
     parts = jnp.stack(three_parts(log_total)).reshape(1, 3 * heads)
     row = jnp.pad(parts, ((0, 15), (0, STATE - 3 * heads)))
-    rows = heads * HEAD_DIM
-    payload = jnp.concatenate([total_state.reshape(rows, STATE), row], axis=0).astype(BF16)
-    gathered = lax.all_gather(payload, "ep")
-    tail = gathered[:, rows, : 3 * heads].astype(F32).reshape(count, 3, heads)
-    logs = jnp.sum(tail, axis=1)
-    at = jnp.arange(count)
-    between = (at[None, :] > at[:, None]) & (at[None, :] < place)
-    spans = jnp.sum(jnp.where(between[:, :, None], logs[None], 0.0), axis=1)
-    weights = jnp.where((at < place)[:, None], jnp.exp(spans), 0.0)
-    wide = jnp.repeat(weights, HEAD_DIM, axis=1)[:, :, None]
-    summed = jnp.sum(gathered[:, :rows, :].astype(F32) * wide, axis=0)
-    return summed.reshape(heads, HEAD_DIM, STATE)
+    payload = jnp.concatenate([total_state.reshape(heads * HEAD_DIM, STATE), row], axis=0)
+    return lax.all_gather(payload.astype(BF16), "ep")
+
+
+def late_kernel(
+    at_ref,
+    g_ref,
+    v_ref,
+    b_ref,
+    c_ref,
+    cum_ref,
+    cum_t_ref,
+    step_t_ref,
+    gate_ref,
+    skip_ref,
+    norm_ref,
+    first_ref,
+    shared_ref,
+    out_ref,
+    mixed_ref,
+):
+    place = at_ref[0]
+    count = g_ref.shape[0]
+    heads = cum_ref.shape[1]
+    rows, width = v_ref.shape
+    top = heads * HEAD_DIM
+    tail = g_ref[:, top, :]
+    row = lax.broadcasted_iota(jnp.int32, (count, count), 0)
+    col = lax.broadcasted_iota(jnp.int32, (count, count), 1)
+    between = jnp.where((col > row) & (col < place), 1.0, 0.0).astype(BF16)
+    parts = jnp.dot(between, tail, preferred_element_type=F32)
+    spans = parts[:, :heads] + parts[:, heads : 2 * heads] + parts[:, 2 * heads : 3 * heads]
+    device = lax.broadcasted_iota(jnp.int32, (count, heads), 0)
+    weights = jnp.where(device < place, jnp.exp(spans), 0.0)
+    pieces = []
+    for h in range(heads):
+        total = jnp.zeros((HEAD_DIM, STATE), F32)
+        for j in range(count):
+            state = g_ref[j, h * HEAD_DIM : (h + 1) * HEAD_DIM, :].astype(F32)
+            total = total + state * weights[j : j + 1, h : h + 1]
+        pieces.append(total)
+    contract = (((1,), (1,)), ((), ()))
+    i = lax.broadcasted_iota(jnp.int32, (BLOCK, BLOCK), 0)
+    j = lax.broadcasted_iota(jnp.int32, (BLOCK, BLOCK), 1)
+    lower = i >= j
+    for block in range(rows // BLOCK):
+        at = slice(block * BLOCK, (block + 1) * BLOCK)
+        c = c_ref[at, :]
+        scores = lax.dot_general(c, b_ref[at, :], contract, preferred_element_type=F32)
+        for h in range(heads):
+            lanes = slice(h * HEAD_DIM, (h + 1) * HEAD_DIM)
+            cum = cum_ref[at, h : h + 1]
+            spread = cum - cum_t_ref[h : h + 1, at]
+            decay = jnp.where(lower, jnp.exp(jnp.where(lower, spread, 0.0)), 0.0)
+            inner = (scores * decay * step_t_ref[h : h + 1, at]).astype(BF16)
+            inside = jnp.dot(inner, v_ref[at, lanes], preferred_element_type=F32)
+            state = pieces[h].astype(BF16)
+            carried = lax.dot_general(c, state, contract, preferred_element_type=F32)
+            mixed_ref[at, lanes] = inside + carried * jnp.exp(cum)
+            if block + 1 < rows // BLOCK:
+                last = jnp.exp(cum_ref[(block + 1) * BLOCK - 1 : (block + 1) * BLOCK, h : h + 1])
+                pieces[h] = pieces[h] * last + first_ref[lanes, :]
+    gate = gate_ref[...].astype(F32)
+    mixed = mixed_ref[...] + skip_ref[...] * v_ref[...].astype(F32)
+    mixed = mixed * (gate / (1.0 + jnp.exp(-gate)))
+    mean = jnp.mean(mixed * mixed, axis=-1, keepdims=True)
+    normed = (mixed * lax.rsqrt(mean + epsilon) * norm_ref[...]).astype(BF16)
+    half = width // 2
+    out_ref[:rows, :] = normed[:, :half]
+    out_ref[rows : 2 * rows, :] = normed[:, half:]
+    out_ref[2 * rows :, :] = jnp.concatenate(
+        [shared_ref[: rows // 2, :], shared_ref[rows // 2 :, :]], axis=1
+    )
+
+
+def late_mixer(place, gathered, v, b, c, cum, cum_t, step_t, gate, skip, norm, first, shared):
+    rows, width = v.shape
+    operands = (gathered, v, b, c, cum, cum_t, step_t, gate, skip, norm, first, shared)
+    return pl.pallas_call(
+        late_kernel,
+        grid=(1,),
+        in_specs=[SCALAR] + [whole(o.shape) for o in operands],
+        out_specs=whole((2 * rows + rows // 2, width // 2)),
+        out_shape=jax.ShapeDtypeStruct((2 * rows + rows // 2, width // 2), BF16),
+        scratch_shapes=[pltpu.VMEM((rows, width), F32)],
+        cost_estimate=pl.CostEstimate(
+            flops=2**28, bytes_accessed=4 * 2**20, transcendentals=2**18
+        ),
+    )(place, *operands)
 
 
 SIDE = 4
@@ -101,8 +182,64 @@
     return jnp.where(i < HALF, half * HALF + i, -7).astype(F32)
 
 
-def pre_kernel(x_ref, g_ref, u_ref, h_ref):
+def dispatch_kernel(at_ref, index_ref, rows_ref, gain_ref, out_ref, normed_ref):
+    y, x = at_ref[0] // SIDE, at_ref[0] % SIDE
+    wide = rows_ref[...].astype(F32)
+    mean = jnp.mean(wide * wide, axis=-1, keepdims=True)
+    normed_ref[...] = (wide * lax.rsqrt(mean + epsilon) * gain_ref[...]).astype(BF16)
+    slots, share = out_ref.shape
+    rows = rows_ref.shape[0]
+    line = lax.broadcasted_iota(jnp.int32, (slots, rows), 0)
+    expert = (line // PADDED) * 2 + y // 2
+    inner = line % PADDED
+    slot = jnp.where(inner < HALF, inner + (y % 2) * HALF, -7)
+    named = index_ref[0:1, :] == expert
+    for k in range(1, TOP_K):
+        named = named | (index_ref[k : k + 1, :] == expert)
+    before = lax.broadcasted_iota(jnp.int32, (rows, rows), 0)
+    after = lax.broadcasted_iota(jnp.int32, (rows, rows), 1)
+    earlier = jnp.where(before < after, 1.0, 0.0).astype(BF16)
+    ones = jnp.where(named, 1.0, 0.0).astype(BF16)
+    place = jnp.dot(ones, earlier, preferred_element_type=F32)
+    taken = named & (place == slot.astype(F32))
+    one_hot = jnp.where(taken, 1.0, 0.0).astype(BF16)
+    mine = normed_ref[:, pl.ds(pl.multiple_of(x * share, share), share)]
+    out_ref[...] = jnp.dot(one_hot, mine, preferred_element_type=F32).astype(BF16)
+
+
+def dispatch(at, index_t, rows, gain, owners):
+    count, width = rows.shape
+    return pl.pallas_call(
+        dispatch_kernel,
+        in_specs=[SCALAR, whole(index_t.shape), whole(rows.shape), whole((1, width))],
+        out_specs=[whole((owners * PADDED, width // SIDE)), whole((count, width))],
+        out_shape=[
+            jax.ShapeDtypeStruct((owners * PADDED, width // SIDE), BF16),
+            jax.ShapeDtypeStruct((count, width), BF16),
+        ],
+        grid=(1,),
+        cost_estimate=pl.CostEstimate(
+            flops=2 * owners * PADDED * count * width // SIDE,
+            bytes_accessed=3 * 2**20,
+            transcendentals=0,
+        ),
+    )(at, index_t, rows, gain.reshape(1, width))
+
+
+def sources(y):
+    return [y, (y + SIDE - 1) % SIDE, (y + 1) % SIDE, (y + 2) % SIDE]
+
+
+def pre_kernel(x_ref, w0_ref, w1_ref, w2_ref, w3_ref, h_ref, g_ref, u_ref):
     k = x_ref.shape[2]
+    ff = w0_ref.shape[0] // 2
+
+    @pl.when(pl.program_id(0) == 0)
+    def _():
+        for j, w_ref in enumerate((w0_ref, w1_ref, w2_ref, w3_ref)):
+            g_ref[j * ff : (j + 1) * ff, :] = w_ref[:ff, :]
+            u_ref[j * ff : (j + 1) * ff, :] = w_ref[ff:, :]
+
     dims = (((1,), (1,)), ((), ()))
     gate = jnp.zeros(h_ref.shape, F32)
     up = jnp.zeros(h_ref.shape, F32)
@@ -115,53 +252,67 @@
     h_ref[...] = (gate / (1.0 + jnp.exp(-gate)) * up).astype(BF16)
 
 
-def expert_hidden(x, g, u):
+def expert_hidden(x, weights):
     slots = x.shape[1]
-    ff, width = g.shape
-    step = 128
+    ff, width = weights[0].shape[0] // 3, weights[0].shape[1]
+    step = 256
     return pl.pallas_call(
         pre_kernel,
         grid=(slots // step,),
-        in_specs=[
-            pl.BlockSpec((SIDE, step, x.shape[2]), lambda i: (0, i, 0)),
-            pl.BlockSpec((ff, width), lambda i: (0, 0)),
-            pl.BlockSpec((ff, width), lambda i: (0, 0)),
-        ],
-        out_specs=pl.BlockSpec((step, ff), lambda i: (i, 0)),
-        out_shape=jax.ShapeDtypeStruct((slots, ff), BF16),
+        in_specs=[pl.BlockSpec((SIDE, step, x.shape[2]), lambda i: (0, i, 0))]
+        + [whole((2 * ff, width))] * SIDE,
+        out_specs=pl.BlockSpec((step, SIDE * ff), lambda i: (i, 0)),
+        out_shape=jax.ShapeDtypeStruct((slots, SIDE * ff), BF16),
+        scratch_shapes=[pltpu.VMEM((SIDE * ff, width), BF16)] * 2,
         cost_estimate=pl.CostEstimate(
-            flops=4 * slots * ff * width, bytes_accessed=4 * 2**20, transcendentals=slots * ff
+            flops=4 * slots * SIDE * ff * width,
+            bytes_accessed=4 * 2**20,
+            transcendentals=slots * SIDE * ff,
         ),
-    )(x, g, u)
-
-
-def down_kernel(h_ref, w_ref, o_ref):
-    k = h_ref.shape[2]
-    for m in range(SIDE):
+    )(x, *weights)
+
+
+def down_kernel(at_ref, h_ref, w0_ref, w1_ref, w2_ref, w3_ref, o_ref):
+    y = at_ref[0] // SIDE
+    order = sources(y)
+    columns = o_ref.shape[2]
+    for owner, w_ref in zip(order, (w0_ref, w1_ref, w2_ref, w3_ref)):
         total = jnp.zeros(o_ref.shape[1:], F32)
         for n in range(SIDE):
-            w = w_ref[m, n * k : (n + 1) * k, :]
+            blocks = [
+                w_ref[:, pl.ds(pl.multiple_of((j * SIDE + n) * columns, columns), columns)]
+                for j in order
+            ]
+            w = jnp.concatenate(blocks, axis=0)
             total = total + jnp.dot(h_ref[n], w, preferred_element_type=F32)
-        o_ref[m] = total.astype(BF16)
-
-
-def expert_down(h, w):
+        o_ref[owner] = total.astype(BF16)
+
+
+def expert_down(at, h, weights):
     slots = h.shape[1]
-    width, columns = w.shape[1:]
-    step = 128
+    ff, width = weights[0].shape[0] // 3, weights[0].shape[1]
+    columns = width // (SIDE * SIDE)
+    step = 256
     return pl.pallas_call(
         down_kernel,
         grid=(slots // step,),
-        in_specs=[
-            pl.BlockSpec((SIDE, step, h.shape[2]), lambda i: (0, i, 0)),
-            pl.BlockSpec(w.shape, lambda i: (0, 0, 0)),
-        ],
+        in_specs=[SCALAR, pl.BlockSpec((SIDE, step, h.shape[2]), lambda i: (0, i, 0))]
+        + [pl.BlockSpec((ff, width), lambda i: (2, 0))] * SIDE,
         out_specs=pl.BlockSpec((SIDE, step, columns), lambda i: (0, i, 0)),
         out_shape=jax.ShapeDtypeStruct((SIDE, slots, columns), BF16),
         cost_estimate=pl.CostEstimate(
-            flops=2 * SIDE * slots * width * columns, bytes_accessed=3 * 2**20, transcendentals=0
+            flops=2 * SIDE * slots * SIDE * SIDE * ff * columns,
+            bytes_accessed=3 * 2**20,
+            transcendentals=0,
         ),
-    )(h, w)
+    )(at, h, *weights)
+
+
+def shifted_down(x, by):
+    pairs = [
+        (SIDE * y + c, SIDE * ((y + by) % SIDE) + c) for y in range(SIDE) for c in range(SIDE)
+    ]
+    return lax.ppermute(x, "tp", pairs)
 
 
 def last_kernel(g_ref, w_ref, s_ref, m_ref, r_ref, m_acc, r_acc):
@@ -226,7 +377,7 @@
     )(gathered, mix_weight, shared_weight)
 
 
-def on_device(
+def step(
     mixer_value_input,
     input_state_matrix,
     output_state_matrix,
@@ -281,82 +432,48 @@
     value_wide = values.astype(F32).reshape(nblocks, BLOCK, heads_local, HEAD_DIM)
     scaled = value_wide * step_length.reshape(nblocks, BLOCK, heads_local)[..., None]
     in_blocks = in_mat.reshape(nblocks, BLOCK, groups_local, STATE)
-    out_blocks = out_mat.reshape(nblocks, BLOCK, groups_local, STATE)
-    scores = jnp.einsum("bign,bjgn->bgij", out_blocks, in_blocks, preferred_element_type=F32)
-    scores = jnp.repeat(scores, head_ratio, axis=1)
-    spread = jnp.transpose(running[:, :, None, :] - running[:, None, :, :], (0, 3, 1, 2))
-    lower_mask = jnp.tril(jnp.ones((BLOCK, BLOCK), bool))[None, None]
-    decay_mat = jnp.where(lower_mask, jnp.exp(jnp.where(lower_mask, spread, 0.0)), 0.0)
-    inside = jnp.einsum("bhij,bjhp->bihp", scores * decay_mat, scaled)
-    out_head = jnp.repeat(out_blocks.astype(F32), head_ratio, axis=2)
     in_head = jnp.repeat(in_blocks.astype(F32), head_ratio, axis=2)
     block_logs = running[:, -1]
     to_end = jnp.exp(block_logs[:, None, :] - running)
     block_state = jnp.einsum("bjhn,bjh,bjhp->bhpn", in_head, to_end, scaled)
     carried = jnp.zeros((heads_local, HEAD_DIM, STATE), F32)
-    before = []
     for b in range(nblocks):
-        before.append(carried)
         carried = carried * jnp.exp(block_logs[b])[:, None, None] + block_state[b]
-    local_prev = jnp.stack(before)
-    before_logs = jnp.cumsum(block_logs, axis=0) - block_logs
-    incoming = state_before(jnp.sum(block_logs, axis=0), carried)
-    entering = local_prev + jnp.exp(before_logs)[:, :, None, None] * incoming[None]
-    carried_term = jnp.einsum("bihn,bhpn->bihp", out_head, entering) * jnp.exp(running)[..., None]
-    mixed_heads = (inside + carried_term).reshape(length, heads_local, HEAD_DIM)
-    mixed_heads = mixed_heads + head_skip_scale[None, :, None] * value_wide.reshape(
-        length, heads_local, HEAD_DIM
-    )
-    gated_heads = mixed_heads * jax.nn.silu(output_gate_input.astype(F32)).reshape(
-        length, heads_local, HEAD_DIM
-    )
-    grouped = gated_heads.reshape(length, groups_local, head_ratio * HEAD_DIM)
-    grouped = grouped * lax.rsqrt(jnp.mean(grouped * grouped, axis=-1, keepdims=True) + epsilon)
-    mixer_normed = (grouped.reshape(length, width_x) * mixer_norm_scale).astype(BF16)
-
-    rows_local = second_token_rows.shape[0]
+    gathered_states = states_gathered(jnp.sum(block_logs, axis=0), carried)
+
     model_width = second_token_rows.shape[1]
     local_experts = routed_gate_weight.shape[0]
     ep_count = lax.axis_size("ep")
     experts = local_experts * ep_count
-    tp_place = lax.axis_index("tp")
-    down, across = tp_place // SIDE, tp_place % SIDE
-    my_expert, my_half = down // 2, down % 2
+    tp_place = lax.axis_index("tp").astype(jnp.int32)
+    at = tp_place.reshape(1)
+    y = tp_place // SIDE
     columns = routed_down_weight.shape[2]
-    part_ff = routed_gate_weight.shape[2]
     share = model_width // SIDE
-
-    gate_up = jnp.stack(
-        [jnp.swapaxes(routed_gate_weight, 1, 2), jnp.swapaxes(routed_up_weight, 1, 2)]
-    )
-    gate_up = jnp.concatenate([gate_up[0], gate_up[1]], axis=1)
-    gate_up = jnp.stack([gate_up[0], gate_up[0], gate_up[1], gate_up[1]])
-    gate_up = along(gate_up, COLUMN_GROUPS)
-    gate_w = gate_up[:, :part_ff].reshape(SIDE * part_ff, model_width)
-    up_w = gate_up[:, part_ff:].reshape(SIDE * part_ff, model_width)
-    down_w = routed_down_weight.reshape(local_experts, SIDE, SIDE, part_ff, columns)
-    down_w = jnp.swapaxes(down_w, 1, 2).reshape(routed_down_weight.shape)
-    down_w = along(jnp.stack([down_w[0], down_w[0], down_w[1], down_w[1]]), COLUMN_GROUPS)
-
-    rows_wide = second_token_rows.astype(F32)
-    normed = (
-        rows_wide
-        * lax.rsqrt(jnp.mean(rows_wide * rows_wide, axis=-1, keepdims=True) + epsilon)
-        * expert_norm_scale
-    ).astype(BF16)
-    place, weight = places(routed_expert_index.T, routed_expert_weight.T, experts)
-    by_owner = place.reshape(ep_count, local_experts, rows_local)
-    mine = lax.dynamic_index_in_dim(by_owner, my_expert, 1, False)
-    taken = mine[:, None, :] == slot_numbers(my_half)[None, :, None]
-    one_hot = taken.astype(BF16).reshape(ep_count * PADDED, rows_local)
-    my_share = lax.dynamic_slice_in_dim(normed, across * share, share, 1)
-    outgoing = jnp.dot(one_hot, my_share, preferred_element_type=F32).astype(BF16)
+    outgoing, normed = dispatch(
+        at, routed_expert_index.T, second_token_rows, expert_norm_scale, ep_count
+    )
     arrived = lax.all_to_all(
         outgoing.reshape(ep_count, PADDED, share), "ep", split_axis=0, concat_axis=0, tiled=True
     )
-    arrived = shown_to_row(arrived.reshape(ep_count * PADDED, share))
-    hidden = shown_to_row(expert_hidden(arrived, gate_w, up_w))
-    result = along(expert_down(hidden, down_w), COLUMN_GROUPS)
+    arrived = arrived.reshape(ep_count * PADDED, share)
+
+    part_ff = routed_gate_weight.shape[2]
+    tall = routed_down_weight.reshape(local_experts, SIDE * SIDE, part_ff, columns)
+    tall = jnp.swapaxes(tall, 1, 2).reshape(local_experts, part_ff, model_width)
+    both = jnp.concatenate(
+        [jnp.swapaxes(routed_gate_weight, 1, 2), jnp.swapaxes(routed_up_weight, 1, 2), tall], axis=1
+    )
+    weights = [lax.dynamic_index_in_dim(both, y // 2, 0, False)]
+    for by in (1, SIDE - 1, 2):
+        goes = lax.dynamic_index_in_dim(both, ((y + by) % SIDE) // 2, 0, False)
+        weights.append(shifted_down(goes, by))
+
+    rows_local = second_token_rows.shape[0]
+    tokens = jnp.broadcast_to(arrived[None], (SIDE,) + arrived.shape)
+    tokens = along(tokens, ROW_GROUPS)
+    hidden = shown_to_row(expert_hidden(tokens, weights))
+    result = along(expert_down(at, hidden, weights), COLUMN_GROUPS)
     result = jnp.swapaxes(result.reshape(SIDE, ep_count, PADDED, columns), 0, 1)
     result = result.reshape(ep_count, SIDE * PADDED, columns)
     returned = lax.all_to_all(result, "ep", split_axis=0, concat_axis=0, tiled=True)
@@ -366,22 +483,29 @@
         jax.nn.silu(jnp.dot(normed, shared_gate_weight, preferred_element_type=F32))
         * jnp.dot(normed, shared_up_weight, preferred_element_type=F32)
     ).astype(BF16)
-    half_rows = rows_local // 2
-    lanes = width_x // 2
-    payload = jnp.concatenate(
-        [
-            mixer_normed[:, :lanes],
-            mixer_normed[:, lanes:],
-            jnp.concatenate([shared_hidden[:half_rows], shared_hidden[half_rows:]], axis=1),
-        ],
-        axis=0,
-    )
-    payload = with_layout_constraint(payload, Layout(major_to_minor=(0, 1)))
+    flat = running.reshape(length, heads_local)
+    payload = late_mixer(
+        lax.axis_index("ep").astype(jnp.int32).reshape(1),
+        gathered_states,
+        values,
+        in_mat,
+        out_mat,
+        flat,
+        flat.T,
+        step_length.T,
+        output_gate_input,
+        jnp.repeat(head_skip_scale, HEAD_DIM)[None, :],
+        mixer_norm_scale[None, :],
+        block_state[0].reshape(heads_local * HEAD_DIM, STATE),
+        shared_hidden,
+    )
     gathered = lax.all_gather(payload, "tp")
     mixer_output, shared_result = last_products(
         gathered, mixer_output_weight, shared_down_weight, rows_local
     )
 
+    place, weight = places(routed_expert_index.T, routed_expert_weight.T, experts)
+    by_owner = place.reshape(ep_count, local_experts, rows_local)
     halves = jnp.stack([slot_numbers(0), slot_numbers(1)])
     taken = by_owner[:, :, None, None, :] == halves[None, None, :, :, None]
     weight = weight.reshape(ep_count, local_experts, 1, 1, rows_local)
@@ -399,7 +523,7 @@
 
 def solution(mesh):
     return jax.shard_map(
-        on_device,
+        step,
         mesh=mesh,
         in_specs=(
             P("ep", "tp"),

time: 271 us -> 261 us (0.963)
  waiting for transfers between devices: 95.2 us -> 119 us
  other arithmetic: 23.9 us -> 7.78 us
  local copies, waits for them, and re-layouts: 24.8 us -> 13.3 us
  blocking collectives: 37.5 us -> 30.4 us
  matrix products: 10.3 us -> 5.54 us
  Pallas kernels: 14.7 us -> 19.1 us
    all_to_all x3 -> x1, waiting for transfers between devices: 38.4 us -> 0.01 us  [along(): lax.all_to_all(x, 'tp', split_axis=0, concat_axis=0, tiled=True, axis_ind...]
    ppermute x0 -> x3, waiting for transfers between devices: none -> 31.5 us  [shifted_down(): return lax.ppermute(x, 'tp', pairs)]
    all_gather x2, waiting for transfers between devices: 28.7 us -> 60 us  [the longest x1 60 us: states_gathered(): return lax.all_gather(payload.astype(BF16), 'ep')]
    ppermute x0 -> x3, starting transfers between devices: none -> 10.3 us  [shifted_down(): return lax.ppermute(x, 'tp', pairs)]
    all_to_all x3 -> x1, starting transfers between devices: 12.4 us -> 3.95 us  [along(): lax.all_to_all(x, 'tp', split_axis=0, concat_axis=0, tiled=True, axis_ind...]
    all_to_all x2, blocking collectives: 37.5 us -> 30.4 us  [along(): lax.all_to_all(x, 'tp', split_axis=0, concat_axis=0, tiled=True, axis_ind...]
    pallas_call x1 -> x3, Pallas kernels: 4.46 us -> 10.7 us  [the longest x1 3.88 us: late_mixer(): pl.pallas_call(late_kernel, grid=(1,), in_specs=[SCALAR] + [whole(o.shape...]
    reduce_sum x6 -> x0, other arithmetic: 5.71 us -> none  [the longest x1 3.18 us: state_before(): summed = jnp.sum(gathered[:, :rows, :].astype(F32) * wide, axis=0)]
  transfers between devices with their start and end apart: 8 -> 9, of which waited for: 5 -> 4; matrix products, arithmetic and copies ran while one was open for 18% -> 6% of each run, Pallas kernels for 5% -> 7%
where the time goes in v3:
time: 261 us; the launch traced here: 260 us
  waiting for transfers between devices  119 us (46%)
  starting transfers between devices  49.4 us (19%)
  blocking collectives  30.4 us (12%)
  Pallas kernels  19.1 us (7%)
  between operations  14.5 us (6%)
  local copies, waits for them, and re-layouts  13.3 us (5%)
  other arithmetic  7.78 us (3%)
  matrix products  5.54 us (2%)
    all_gather x1, waiting for transfers between devices, states_gathered(): return lax.all_gather(payload.astype(BF16), 'ep')  60 us
    ppermute x3, waiting for transfers between devices, shifted_down(): return lax.ppermute(x, 'tp', pairs)  31.5 us
    all_to_all x2, blocking collectives, along(): lax.all_to_all(x, 'tp', split_axis=0, concat_axis=0, tiled=True, axis_ind...  30.4 us
    all_to_all x1, waiting for transfers between devices, step(): lax.all_to_all(result, 'ep', split_axis=0, concat_axis=0, tiled=True)  27.9 us
    all_to_all x1, starting transfers between devices, step(): lax.all_to_all(result, 'ep', split_axis=0, concat_axis=0, tiled=True)  15.6 us
    all_to_all x1, starting transfers between devices, step(): lax.all_to_all(outgoing.reshape(ep_count, PADDED, share), 'ep', split_axi...  14.6 us
    ppermute x3, starting transfers between devices, shifted_down(): return lax.ppermute(x, 'tp', pairs)  10.3 us
  transfers between devices with their start and end apart: 9, of which 4 were waited for; matrix products, arithmetic and copies ran while one was open for 6% of the time, Pallas kernels for 7%

profile of v3, /device:TPU:1, one launch (start us, length us, event | category | flops | bytes accessed | tf_op | source)
XLA Modules:
  0.0 259.5 jit_solution(17733251413840152991)
XLA Ops:
  7.2 0.7 slice.128
  8.0 0.7 slice.129
  8.6 0.7 slice.127
  9.3 4.9 %collective-permute-start = (bf16[3,512]{1,0:T(4,128)(2,1)S(1)}, bf16[3,512]{1,0:T(4,128)(2,1)S(1)}, u32[]{:S(2)}, u32[]{:S(2)}) collective-permute-start(bf16[3,512]{1,0:T(4,128)(2,1)S(1)} %pad_maximum_fusion.5), channel_id=1, source_target_pairs={{0,16},{16,32},{32,48},{48,64},{64,80},{80,96},{96,112},{112,128},... | collective-permute-start | bytes 9224 | tf_op jit(solution)/shard_map/ppermute | solution.py:28
  14.3 0.7 exponential_negate_fusion
  14.9 1.3 fusion.31
  16.4 0.2 reduce_window_sum.11
  16.6 0.8 slice_bitcast_fusion.7
  17.5 0.8 fusion.38
  18.9 1.4 multiply_convert_fusion.v_ref
  20.4 0.1 reshape.446
  20.9 0.2 fusion.4
  21.1 0.1 fusion.9
  21.3 0.6 pad_maximum_fusion.2
  21.9 3.1 %shard_map.230 = (bf16[512,512]{1,0:T(8,128)(2,1)}, bf16[256,2048]{1,0:T(8,128)(2,1)}) custom-call(s32[1]{0:T(128)} %bitcast.27.at_ref, s32[4,256]{1,0:T(4,128)} %bitcast.120, bf16[256,2048]{1,0:T(8,128)(2,1)} %rows_ref.1, f32[1,2048]{1,0:T(1,128)} %bitcast.122), custom_call_target="tpu_custom_call" | custom-call | flops 134217728 | bytes 3145728 | tf_op jit(solution)/shard_map/pallas_call | solution.py:212
  25.0 14.6 %all-to-all-start = ((bf16[32,16,512]{2,1,0:T(8,128)(2,1)}), bf16[32,16,512]{2,1,0:T(8,128)(2,1)S(1)}, u32[]{:S(2)}, u32[]{:S(2)}) async-start(bf16[32,16,512]{2,1,0:T(8,128)(2,1)} %bitcast.114), calls=%async_computation | async-start | bytes 1048576 | tf_op jit(solution)/shard_map/all_to_all | solution.py:456
  39.8 0.7 broadcast_in_dim_reshape.2.skip_ref
  40.4 0.7 copy.73
  41.1 1.6 fusion.39
  42.8 1.1 fusion.2.shared_ref
  43.9 0.7 multiply_convert_fusion.1.c_ref
  44.6 60.0 %all-gather.4.cloned.1.call-done.g_ref = bf16[32,272,128]{2,1,0:T(8,128)(2,1)} async-done(((bf16[1,272,128]{2,1,0:T(8,128)(2,1)}), bf16[32,272,128]{2,1,0:T(8,128)(2,1)}) %all-gather.4.cloned.1.call-update) | async-done | bytes 2228240 | tf_op jit(solution)/shard_map/all_gather | solution.py:58
  104.6 3.9 %shard_map.231 = bf16[640,128]{1,0:T(8,128)(2,1)} custom-call(s32[1]{0:T(128)} %bitcast.at_ref, bf16[32,272,128]{2,1,0:T(8,128)(2,1)} %all-gather.4.cloned.1.call-done.g_ref, bf16[256,256]{1,0:T(8,128)(2,1)} %copy-done.5, bf16[256,128]{1,0:T(8,128)(2,1)} %copy-done.8, bf16[256,128]{1,0:T(8,128)(2,1)} %multiply_convert_fusion.1.c_ref, f32[256,4]{1,0:T(8,128)} %bitcast.107, ...), custom_call_target="tpu_custom_call" | custom-call | flops 268435456 | bytes 4194304 | tf_op jit(solution)/shard_map/pallas_call | solution.py:135
  108.5 1.5 broadcast_in_dim.112
  110.0 3.9 %all-to-all-start.1 = ((bf16[4,512,512]{2,1,0:T(8,128)(2,1)}), bf16[4,512,512]{2,1,0:T(8,128)(2,1)S(1)}, u32[]{:S(2)}, u32[]{:S(2)}) async-start(bf16[4,512,512]{2,1,0:T(8,128)(2,1)} %broadcast_in_dim.112), calls=%async_computation.1 | async-start | bytes 4194304 | tf_op jit(solution)/shard_map/all_to_all | solution.py:156
  114.1 1.3 pad_maximum_fusion
  115.4 1.3 dynamic-slice_bitcast_fusion
  116.7 5.0 %collective-permute-start.3 = (bf16[192,2048]{1,0:T(8,128)(2,1)S(1)}, bf16[192,2048]{1,0:T(8,128)(2,1)S(1)}, u32[]{:S(2)}, u32[]{:S(2)}) collective-permute-start(bf16[192,2048]{1,0:T(8,128)(2,1)S(1)} %get-tuple-element.10), channel_id=1, source_target_pairs={{0,8},{1,9},{2,10},{3,11},{4,12},{5,13},{6,14},{7,15},{8,0},{9,1},... | collective-permute-start | bytes 2359304 | tf_op jit(solution)/shard_map/ppermute | solution.py:315
  121.8 3.0 %collective-permute-start.2 = (bf16[192,2048]{1,0:T(8,128)(2,1)S(1)}, bf16[192,2048]{1,0:T(8,128)(2,1)S(1)}, u32[]{:S(2)}, u32[]{:S(2)}) collective-permute-start(bf16[192,2048]{1,0:T(8,128)(2,1)S(1)} %get-tuple-element.11), channel_id=1, source_target_pairs={{0,12},{1,13},{2,14},{3,15},{4,0},{5,1},{6,2},{7,3},{8,4},{9,5},{1... | collective-permute-start | bytes 2359304 | tf_op jit(solution)/shard_map/ppermute | solution.py:315
  124.7 2.3 collective-permute-start.1
  127.1 14.1 %collective-permute-done.3.w3_ref = bf16[192,2048]{1,0:T(8,128)(2,1)S(1)} collective-permute-done((bf16[192,2048]{1,0:T(8,128)(2,1)S(1)}, bf16[192,2048]{1,0:T(8,128)(2,1)S(1)}, u32[]{:S(2)}, u32[]{:S(2)}) %collective-permute-start.3) | collective-permute-done | bytes 786464 | tf_op jit(solution)/shard_map/ppermute | solution.py:315
  141.1 17.4 %collective-permute-done.2.w2_ref = bf16[192,2048]{1,0:T(8,128)(2,1)S(1)} collective-permute-done((bf16[192,2048]{1,0:T(8,128)(2,1)S(1)}, bf16[192,2048]{1,0:T(8,128)(2,1)S(1)}, u32[]{:S(2)}, u32[]{:S(2)}) %collective-permute-start.2) | collective-permute-done | bytes 786464 | tf_op jit(solution)/shard_map/ppermute | solution.py:315
  158.6 0.9 copy-done.3
  159.5 1.3 copy-done.1
  160.8 4.2 %shard_map.233 = bf16[512,256]{1,0:T(8,128)(2,1)} custom-call(bf16[4,512,512]{2,1,0:T(8,128)(2,1)} %copy-done.1, bf16[192,2048]{1,0:T(8,128)(2,1)} %get-tuple-element.13.w0_ref, bf16[192,2048]{1,0:T(8,128)(2,1)} %collective-permute-done.1.w1_ref, bf16[192,2048]{1,0:T(8,128)(2,1)} %copy-done.3, bf16[192,2048]{1,0:T(8,128)(2,1)} %copy-done.2), custom_call_target="tpu_custom_call" | custom-call | flops 1073741824 | bytes 4194304 | tf_op jit(solution)/shard_map/pallas_call | solution.py:259
  165.0 1.0 broadcast_in_dim.113
  166.1 18.9 %all_to_all.25.h_ref = bf16[4,512,256]{2,1,0:T(8,128)(2,1)} all-to-all(bf16[4,512,256]{2,1,0:T(8,128)(2,1)S(1)} %broadcast_in_dim.113), channel_id=1, replica_groups={{0,1,2,3},{4,5,6,7},{8,9,10,11},{12,13,14,15},{16,17,18,19},{20,21,22,2..., dimensions={0} | all-to-all | bytes 2097152 | tf_op jit(solution)/shard_map/all_to_all | solution.py:156
  185.0 3.7 %shard_map.234 = bf16[4,512,128]{2,1,0:T(8,128)(2,1)} custom-call(s32[1]{0:T(128)} %bitcast.27.at_ref, bf16[4,512,256]{2,1,0:T(8,128)(2,1)} %all_to_all.25.h_ref, bf16[192,2048]{1,0:T(8,128)(2,1)} %get-tuple-element.13.w0_ref, bf16[192,2048]{1,0:T(8,128)(2,1)} %collective-permute-done.1.w1_ref, bf16[192,2048]{1,0:T(8,128)(2,1)} %copy-done.3, ...), custom_call_target="tpu_custom_call" | custom-call | flops 536870912 | bytes 3145728 | tf_op jit(solution)/shard_map/pallas_call | solution.py:296
  188.7 11.5 %all_to_all.26 = bf16[4,512,128]{2,1,0:T(8,128)(2,1)S(1)} all-to-all(bf16[4,512,128]{2,1,0:T(8,128)(2,1)} %shard_map.234), channel_id=1, replica_groups={{0,4,8,12},{1,5,9,13},{2,6,10,14},{3,7,11,15},{16,20,24,28},{17,21,25,2..., dimensions={0} | all-to-all | bytes 1048576 | tf_op jit(solution)/shard_map/all_to_all | solution.py:156
  200.2 0.9 copy.69
  201.1 15.6 %all-to-all-start.4 = ((bf16[32,64,128]{2,1,0:T(8,128)(2,1)}), bf16[32,64,128]{2,1,0:T(8,128)(2,1)S(1)}, u32[]{:S(2)}, u32[]{:S(2)}) async-start(bf16[32,64,128]{2,1,0:T(8,128)(2,1)} %bitcast.53), calls=%async_computation.4 | async-start | bytes 1048576 | tf_op jit(solution)/shard_map/all_to_all | solution.py:479
  216.7 0.2 convolution_select_fusion
  217.0 0.2 reduce-precision_subtract_fusion
  217.1 0.9 fusion.1
  218.0 4.2 %shard_map.232 = (bf16[256,128]{1,0:T(8,128)(2,1)}, f32[256,128]{1,0:T(8,128)}) custom-call(bf16[16,640,128]{2,1,0:T(8,128)(2,1)} %bitcast.105, bf16[4096,128]{1,0:T(8,128)(2,1)} %w_ref.1, bf16[1024,128]{1,0:T(8,128)(2,1)} %s_ref.1), custom_call_target="tpu_custom_call" | custom-call | flops 335544320 | bytes 4194304 | tf_op jit(solution)/shard_map/pallas_call | solution.py:355
  222.3 27.9 %all-to-all-done.4 = bf16[32,64,128]{2,1,0:T(8,128)(2,1)S(1)} async-done(((bf16[32,64,128]{2,1,0:T(8,128)(2,1)}), bf16[32,64,128]{2,1,0:T(8,128)(2,1)S(1)}, u32[]{:S(2)}, u32[]{:S(2)}) %all-to-all-start.4) | async-done | bytes 524320 | tf_op jit(solution)/shard_map/all_to_all | solution.py:479
  250.2 1.4 convolution_add_fusion.1
  251.6 1.1 fusion.3
  (71 shorter events, 1.5 us)
Async XLA Ops:
  7.2 34.0 %copy-start = (bf16[2048,64]{0,1:T(8,128)(2,1)S(1)}, bf16[2048,64]{0,1:T(8,128)(2,1)}, u32[]{:S(2)}) copy-start(bf16[2048,64]{0,1:T(8,128)(2,1)} %param.43) | copy-start | bytes 786436
  7.2 13.5 %copy-start.10 = (bf16[256,128]{1,0:T(8,128)(2,1)S(1)}, bf16[256,128]{1,0:T(8,128)(2,1)}, u32[]{:S(2)}) copy-start(bf16[256,128]{1,0:T(8,128)(2,1)} %param.24) | copy-start | bytes 196612
  7.2 97.4 %all-gather.4.cloned.1.call-start = ((), (), s32[]{:S(2)}) async-start(), calls=%async_computation.5 | async-start | bytes 2297856 | tf_op jit(solution)/shard_map/all_gather | solution.py:58
  9.3 9.5 %collective-permute-start = (bf16[3,512]{1,0:T(4,128)(2,1)S(1)}, bf16[3,512]{1,0:T(4,128)(2,1)S(1)}, u32[]{:S(2)}, u32[]{:S(2)}) collective-permute-start(bf16[3,512]{1,0:T(4,128)(2,1)S(1)} %pad_maximum_fusion.5), channel_id=1, source_target_pairs={{0,16},{16,32},{32,48},{48,64},{64,80},{80,96},{96,112},{112,128},... | collective-permute-start | bytes 9224 | tf_op jit(solution)/shard_map/ppermute | solution.py:28
  16.6 23.8 %copy-start.4 = (f32[2,128,4]{2,1,0:T(8,128)}, f32[2,128,4]{2,1,0:T(8,128)S(1)}, u32[]{:S(2)}) copy-start(f32[2,128,4]{2,1,0:T(8,128)S(1)} %reduce_window_sum.11) | copy-start | bytes 12292
  20.3 4.7 %copy-start.5 = (bf16[256,256]{1,0:T(8,128)(2,1)}, bf16[256,256]{1,0:T(8,128)(2,1)S(1)}, u32[]{:S(2)}) copy-start(bf16[256,256]{1,0:T(8,128)(2,1)S(1)} %multiply_convert_fusion.v_ref) | copy-start | bytes 393220
  20.6 19.1 %copy-start.15 = (f32[4]{0:T(128)S(1)}, f32[4]{0:T(128)}, u32[]{:S(2)}) copy-start(f32[4]{0:T(128)} %param.30) | copy-start | bytes 52
  20.6 20.5 %copy-start.14 = (f32[4,128]{1,0:T(4,128)S(1)}, f32[4,128]{1,0:T(4,128)}, u32[]{:S(2)}) copy-start(f32[4,128]{1,0:T(4,128)} %param.33) | copy-start | bytes 6148
  20.8 21.9 %copy-start.8 = (bf16[256,128]{1,0:T(8,128)(2,1)}, bf16[256,128]{1,0:T(8,128)(2,1)S(1)}, u32[]{:S(2)}) copy-start(bf16[256,128]{1,0:T(8,128)(2,1)S(1)} %multiply_convert_fusion.2.b_ref) | copy-start | bytes 196612
  21.1 21.7 %copy-start.6 = (f32[1,4,64,128]{3,2,1,0:T(8,128)}, f32[1,4,64,128]{3,2,1,0:T(8,128)S(1)}, u32[]{:S(2)}) copy-start(f32[1,4,64,128]{3,2,1,0:T(8,128)S(1)} %get-tuple-element.14) | copy-start | bytes 393220
  21.1 21.7 %copy-start.16 = (bf16[2048,64]{0,1:T(8,128)(2,1)S(1)}, bf16[2048,64]{0,1:T(8,128)(2,1)}, u32[]{:S(2)}) copy-start(bf16[2048,64]{0,1:T(8,128)(2,1)} %param.44) | copy-start | bytes 786436
  25.0 17.8 %copy-start.7 = (bf16[256,2048]{1,0:T(8,128)(2,1)S(1)}, bf16[256,2048]{1,0:T(8,128)(2,1)}, u32[]{:S(2)}) copy-start(bf16[256,2048]{1,0:T(8,128)(2,1)} %get-tuple-element.6) | copy-start | bytes 3145732
  25.0 18.9 %copy-start.11 = (bf16[256,128]{1,0:T(8,128)(2,1)S(1)}, bf16[256,128]{1,0:T(8,128)(2,1)}, u32[]{:S(2)}) copy-start(bf16[256,128]{1,0:T(8,128)(2,1)} %param.25) | copy-start | bytes 196612
  25.0 83.4 %all-to-all-start = ((bf16[32,16,512]{2,1,0:T(8,128)(2,1)}), bf16[32,16,512]{2,1,0:T(8,128)(2,1)S(1)}, u32[]{:S(2)}, u32[]{:S(2)}) async-start(bf16[32,16,512]{2,1,0:T(8,128)(2,1)} %bitcast.114), calls=%async_computation | async-start | bytes 1048576 | tf_op jit(solution)/shard_map/all_to_all | solution.py:456
  39.6 178.4 %all-gather.6.cloned.1.call-start = ((), (), s32[]{:S(2)}) async-start(), calls=%async_computation.6 | async-start | bytes 2785280 | tf_op jit(solution)/shard_map/all_gather | solution.py:502
  110.0 4.0 %copy-start.9 = (bf16[2,1024,128]{2,1,0:T(8,128)(2,1)S(1)}, bf16[2,1024,128]{2,1,0:T(8,128)(2,1)}, u32[]{:S(2)}) copy-start(bf16[2,1024,128]{2,1,0:T(8,128)(2,1)} %param.42) | copy-start | bytes 1572868
  110.0 49.5 %all-to-all-start.1 = ((bf16[4,512,512]{2,1,0:T(8,128)(2,1)}), bf16[4,512,512]{2,1,0:T(8,128)(2,1)S(1)}, u32[]{:S(2)}, u32[]{:S(2)}) async-start(bf16[4,512,512]{2,1,0:T(8,128)(2,1)} %broadcast_in_dim.112), calls=%async_computation.1 | async-start | bytes 4194304 | tf_op jit(solution)/shard_map/all_to_all | solution.py:156
  116.7 24.4 %collective-permute-start.3 = (bf16[192,2048]{1,0:T(8,128)(2,1)S(1)}, bf16[192,2048]{1,0:T(8,128)(2,1)S(1)}, u32[]{:S(2)}, u32[]{:S(2)}) collective-permute-start(bf16[192,2048]{1,0:T(8,128)(2,1)S(1)} %get-tuple-element.10), channel_id=1, source_target_pairs={{0,8},{1,9},{2,10},{3,11},{4,12},{5,13},{6,14},{7,15},{8,0},{9,1},... | collective-permute-start | bytes 2359304 | tf_op jit(solution)/shard_map/ppermute | solution.py:315
  121.8 36.8 %collective-permute-start.2 = (bf16[192,2048]{1,0:T(8,128)(2,1)S(1)}, bf16[192,2048]{1,0:T(8,128)(2,1)S(1)}, u32[]{:S(2)}, u32[]{:S(2)}) collective-permute-start(bf16[192,2048]{1,0:T(8,128)(2,1)S(1)} %get-tuple-element.11), channel_id=1, source_target_pairs={{0,12},{1,13},{2,14},{3,15},{4,0},{5,1},{6,2},{7,3},{8,4},{9,5},{1... | collective-permute-start | bytes 2359304 | tf_op jit(solution)/shard_map/ppermute | solution.py:315
  124.7 34.8 %collective-permute-start.1 = (bf16[192,2048]{1,0:T(8,128)(2,1)S(1)}, bf16[192,2048]{1,0:T(8,128)(2,1)}, u32[]{:S(2)}, u32[]{:S(2)}) collective-permute-start(bf16[192,2048]{1,0:T(8,128)(2,1)S(1)} %get-tuple-element.12), channel_id=1, source_target_pairs={{0,4},{1,5},{2,6},{3,7},{4,8},{5,9},{6,10},{7,11},{8,12},{9,13},{1... | collective-permute-start | bytes 2359304 | tf_op jit(solution)/shard_map/ppermute | solution.py:315
  141.1 18.3 %copy-start.2 = (bf16[192,2048]{1,0:T(8,128)(2,1)}, bf16[192,2048]{1,0:T(8,128)(2,1)S(1)}, u32[]{:S(2)}) copy-start(bf16[192,2048]{1,0:T(8,128)(2,1)S(1)} %collective-permute-done.3.w3_ref) | copy-start | bytes 2359300
  158.6 0.9 copy-start.3
  159.5 1.4 copy-start.1
  188.7 28.0 %copy-start.12 = (s32[256,4]{0,1:T(4,128)S(1)}, s32[256,4]{0,1:T(4,128)}, u32[]{:S(2)}) copy-start(s32[256,4]{0,1:T(4,128)} %param.38) | copy-start | bytes 12292
  188.7 28.2 %copy-start.13 = (f32[256,4]{0,1:T(4,128)S(1)}, f32[256,4]{0,1:T(4,128)}, u32[]{:S(2)}) copy-start(f32[256,4]{0,1:T(4,128)} %param.39) | copy-start | bytes 12292
  201.1 49.1 %all-to-all-start.4 = ((bf16[32,64,128]{2,1,0:T(8,128)(2,1)}), bf16[32,64,128]{2,1,0:T(8,128)(2,1)S(1)}, u32[]{:S(2)}, u32[]{:S(2)}) async-start(bf16[32,64,128]{2,1,0:T(8,128)(2,1)} %bitcast.53), calls=%async_computation.4 | async-start | bytes 1048576 | tf_op jit(solution)/shard_map/all_to_all | solution.py:479
Sparse Core Ops, SparseCore 0:
  22.0 82.4 all-gather.3
  108.6 65.5 all-gather.5
